TPU v7x, 32 devices: a whole 2x2x4 slice. The times are simulated.
32 devices in a mesh: sp: 8 (over z, core), tp: 4 (over y, x).
Axes of the slice: x: 2, y: 2, z: 4, core: 2. Of those that a mesh axis runs over, the one named last changes fastest.
Arguments:
- tokens: bfloat16 [2048, 4096], P('sp'), may hold values from -6 to 6
- norm_gain: float32 [2, 4096], replicated, may hold values from 0.1 to 1.9
- w_outer: bfloat16 [2, 4096, 1024], P(None, 'sp', 'tp'), may hold values from -0.09375 to 0.09375
- w_inner: bfloat16 [2, 4096, 1024], P(None, 'sp', 'tp'), may hold values from -0.09375 to 0.09375
- w_value: bfloat16 [2, 4096, 1024], P(None, 'sp', 'tp'), may hold values from -0.09375 to 0.09375
- w_back: bfloat16 [2, 1024, 4096], P(None, 'sp', 'tp'), may hold values from -0.1875 to 0.1875
- taps: float32 [2, 3, 1024], P(None, None, 'tp'), may hold values from -3 to 3
Outputs:
- result: bfloat16 [2048, 4096], P('sp', 'tp')
All inputs are finite; a program needn't handle non-finite values.
Results may differ from a plain program's by a relative error of at most 0.022.
Values may be sent and summed in bfloat16 or wider, within the bound.
A program may use at most 64 MiB of HBM per device.

v0:
```python
import functools

import jax
import jax.numpy as jnp
from jax import lax
from jax.experimental import pallas as pl
from jax.experimental.pallas import tpu as pltpu
from jax.sharding import PartitionSpec as P

MESH = pl.DeviceIdType.MESH
f32 = jnp.float32
bf16 = jnp.bfloat16

eps = 1e-06


def shifted(block, axis, distance):
    devices = range(lax.axis_size(axis))
    route = [(i - distance, i) for i in devices if i - distance in devices]
    return lax.ppermute(block, axis, route)


def per_device(tokens, norm_gain, w_outer, w_inner, w_value, w_back, taps):
    layers = w_outer.shape[0]
    count = tokens.shape[0]
    feats = w_back.shape[2]
    own = lax.axis_index("tp")
    held = (
        lax.all_gather(w_outer, "sp", axis=1, tiled=True),
        lax.all_gather(w_inner, "sp", axis=1, tiled=True),
        lax.all_gather(w_value, "sp", axis=1, tiled=True),
        lax.all_gather(w_back, "sp", axis=1, tiled=True),
    )
    current = tokens
    resid = lax.dynamic_slice_in_dim(tokens, own * feats, feats, 1)
    for layer in range(layers):
        if layer > 0:
            current = lax.all_gather(resid, "tp", axis=1, tiled=True)
        xf = current.astype(jnp.float32)
        normed = (
            xf * lax.rsqrt(jnp.mean(xf * xf, axis=-1, keepdims=True) + eps) * norm_gain[layer]
        ).astype(jnp.bfloat16)
        outer = jnp.dot(normed, held[0][layer], preferred_element_type=jnp.float32)
        inner = jnp.dot(normed, held[1][layer], preferred_element_type=jnp.float32)
        value = jnp.dot(normed, held[2][layer], preferred_element_type=jnp.float32)
        outer = outer.astype(jnp.bfloat16)
        inner = inner.astype(jnp.bfloat16)
        value = value.astype(jnp.bfloat16)
        mixed = (inner.astype(jnp.float32) * value.astype(jnp.float32)).astype(jnp.bfloat16)
        before = shifted(mixed[count - 2 :], "sp", 1)
        padded = jnp.concatenate([before, mixed], axis=0).astype(jnp.float32)
        conv = (
            taps[layer, 0] * padded[:count]
            + taps[layer, 1] * padded[1 : count + 1]
            + taps[layer, 2] * padded[2:]
        )
        gated = (outer.astype(jnp.float32) * conv).astype(jnp.bfloat16)
        whole = lax.all_gather(gated, "tp", axis=1, tiled=True)
        proj = jnp.dot(whole, held[3][layer], preferred_element_type=jnp.float32)
        resid = (resid.astype(jnp.float32) + proj).astype(jnp.bfloat16)
    return resid


def mixer_kernel(
    tok, gain, w_outer, w_inner, w_value, w_back, taps, out,
    xs, win, wback, acc, ss, gat, mixed, halo, res, landed,
    sem_local, sem_tok_local, tok_send, tok_recv, w_send, w_recv,
    g_send, g_recv, h_send, h_recv, o_send, o_recv,
):
    s, t = lax.axis_index("sp"), lax.axis_index("tp")
    n_sp, n_tp = win.shape[1], xs.shape[1]
    layers = wback.shape[0]
    rows = tok.shape[0]
    feats = xs.shape[3]
    units = 4 * layers
    core = lax.rem(s, 2)
    flip = 1 - 2 * core
    left = s < n_sp // 2
    side = jnp.where(left, 1, -1)
    plane = lax.div(s, 2)
    is_end = jnp.logical_or(plane == 0, plane == n_sp // 2 - 1)
    is_mid = jnp.logical_not(is_end)
    partner = s + flip
    inward = jnp.where(is_end, s + 2 * side, s)
    end = jnp.where(is_mid, s - 2 * side, s)
    opp = jnp.where(is_mid, s + 2 * side, s)
    oppend = jnp.where(is_mid, s + 4 * side, s)
    tx = t + 1 - 2 * lax.rem(t, 2)
    ty = t + 2 - 4 * lax.div(t, 2)
    td = n_tp - 1 - t

    barrier = pltpu.get_barrier_semaphore()
    for k in range(1, n_sp):
        pl.semaphore_signal(barrier, inc=1, device_id=(lax.rem(s + k, n_sp), t), device_id_type=MESH)
    for other in (tx, ty):
        pl.semaphore_signal(barrier, inc=1, device_id=(s, other), device_id_type=MESH)
    pl.semaphore_wait(barrier, n_sp + 1)

    projections = (w_outer, w_inner, w_value)

    def own_w(u):
        layer, m = u // 4, u % 4
        return projections[m].at[layer] if m < 3 else w_back.at[layer]

    def held_w(u, source):
        layer, m = u // 4, u % 4
        return win.at[3 * layer + m, source] if m < 3 else wback.at[layer, source]

    def remote(a, b, ssem, rsem, sp, tp):
        return pltpu.make_async_remote_copy(
            src_ref=a, dst_ref=b, send_sem=ssem, recv_sem=rsem, device_id=(sp, tp), device_id_type=MESH
        )

    def send_w(u, source, kind, target, own=False):
        a = own_w(u) if own else held_w(u, source)
        remote(a, held_w(u, source), w_send.at[u, kind], w_recv.at[u, source], target, t).start()

    def wait_w(u, source):
        remote(held_w(u, source), held_w(u, source), w_send.at[u, 0], w_recv.at[u, source], partner, t).wait_recv()

    def tok_cols(j):
        return tok.at[:, pl.ds(pl.multiple_of(j * feats, feats), feats)]

    def tok_to_end_mid():
        target = lax.div(s, 2) + 2
        place = xs.at[0, t, pl.ds(pl.multiple_of(core * rows, rows), rows)]
        return remote(tok_cols(t), place, tok_send.at[0], tok_recv.at[core], target, t)

    outer_mid = jnp.logical_or(s == 2, s == n_sp - 3)
    my_half = pl.multiple_of(jnp.where(left, 1, 0) * rows, rows)
    partner_half = pl.multiple_of(jnp.where(left, 0, 1) * rows, rows)

    def tok_local(j):
        return pltpu.make_async_copy(tok_cols(j), xs.at[0, j, pl.ds(my_half, rows)], sem_tok_local.at[j])

    def tok_partner(j):
        return remote(tok_cols(j), xs.at[0, j, pl.ds(partner_half, rows)], tok_send.at[j], tok_recv.at[j], partner, t)

    def result_copy(b):
        return remote(res.at[b], landed, o_send.at[b], o_recv, 2 * (s - 2) + b, t)

    def result_wait():
        remote(landed, landed, o_send.at[0], o_recv, partner, t).wait_recv()
        out[...] = landed[...]

    @pl.when(is_end)
    def _():
        sends = []
        for u in range(units):
            send_w(u, s, 0, inward, own=True)
            if u == 0:
                tok_to_end_mid().start()
        for u in range(units):
            remote(own_w(u), held_w(u, s), w_send.at[u, 0], w_recv.at[u, s], inward, t).wait_send()
        tok_to_end_mid().wait_send()
        result_wait()

    def gather_pieces(g, buf):
        size = buf.shape[1] // 2
        def piece(block, half, k, target):
            ref = buf.at[block, pl.ds(half * size, size)]
            return remote(ref, ref, g_send.at[g, k], g_recv.at[g, k], s, target)
        return piece

    def gather_start(g, buf):
        p = gather_pieces(g, buf)
        p(t, 0, 0, tx).start()
        p(t, 1, 1, ty).start()
        p(t, 1, 2, tx).start()
        p(t, 0, 3, ty).start()

    def gather_forward(g, buf):
        p = gather_pieces(g, buf)
        p(tx, 0, 0, tx).wait_recv()
        p(tx, 0, 4, ty).start()
        p(ty, 1, 1, ty).wait_recv()
        p(ty, 1, 5, tx).start()

    def gather_near(g, buf):
        p = gather_pieces(g, buf)
        p(tx, 1, 2, tx).wait_recv()
        p(ty, 0, 3, ty).wait_recv()

    def gather_far(g, buf):
        p = gather_pieces(g, buf)
        p(td, 0, 4, ty).wait_recv()
        p(td, 1, 5, tx).wait_recv()

    def gather_drain(g, buf):
        p = gather_pieces(g, buf)
        p(t, 0, 0, tx).wait_send()
        p(t, 1, 1, ty).wait_send()
        p(t, 1, 2, tx).wait_send()
        p(t, 0, 3, ty).wait_send()
        p(tx, 0, 4, ty).wait_send()
        p(ty, 1, 5, tx).wait_send()

    def take_end(u):
        wait_w(u, end)
        send_w(u, end, 2, opp)
        send_w(u, end, 3, partner)

    def pump(u):
        if u + 1 < units:
            take_end(u + 1)
        if u + 4 < units:
            send_w(u + 4, s, 0, opp, own=True)
        wait_w(u, opp)
        send_w(u, opp, 4, partner)
        wait_w(u, oppend)
        send_w(u, oppend, 5, partner)

    def settle(u):
        pltpu.make_async_copy(own_w(u), held_w(u, s), sem_local.at[u]).wait()
        for source in (s, end, opp, oppend):
            wait_w(u, source + flip)

    def project(layer, j, first):
        def tile(r, carry):
            span = pl.ds(pl.multiple_of(r * rows, rows), rows)
            x = xs[layer, j, span, :].astype(f32)
            sq = x * x
            part = sq[:, :128]
            for q in range(1, feats // 128):
                part = part + sq[:, 128 * q : 128 * (q + 1)]
            scaled = (x * gain[layer : layer + 1, pl.ds(pl.multiple_of(j * feats, feats), feats)]).astype(bf16)
            depth = win.shape[2]
            per = feats // depth
            dots = []
            for m in range(3):
                w = win[3 * layer + m, pl.ds(per * j, per)].reshape(feats, win.shape[3])
                dots.append(jnp.dot(scaled, w, preferred_element_type=f32))
            if first:
                ss[span, :] = part
                for m in range(3):
                    acc[m, span, :] = dots[m]
            else:
                ss[span, :] += part
                for m in range(3):
                    acc[m, span, :] += dots[m]
            return carry
        lax.fori_loop(0, 2, tile, 0)

    def halo_copy(layer):
        count = 2 * rows
        return remote(
            mixed.at[pl.ds(count - 16, 16)], halo.at[layer], h_send.at[layer], h_recv.at[layer], s + 1, t
        )

    def gate(layer):
        width = feats * n_tp
        inv = lax.rsqrt(jnp.sum(ss[...], axis=-1, keepdims=True) / width + eps)
        inner = (acc[1] * inv).astype(bf16)
        value = (acc[2] * inv).astype(bf16)
        mix = (inner.astype(f32) * value.astype(f32)).astype(bf16)
        if layer > 0:
            @pl.when(s < n_sp - 3)
            def _():
                halo_copy(layer - 1).wait_send()
        mixed[...] = mix
        @pl.when(s < n_sp - 3)
        def _():
            halo_copy(layer).start()
        outer = (acc[0] * inv).astype(bf16).astype(f32)
        @pl.when(s == 2)
        def _():
            halo[layer] = jnp.zeros(halo.shape[1:], bf16)
        @pl.when(s > 2)
        def _():
            halo_copy(layer).wait_recv()
        now = mix.astype(f32)
        tail = halo[layer].astype(f32)
        row = lax.broadcasted_iota(jnp.int32, now.shape, 0)
        one = jnp.where(row == 0, tail[15:16], pltpu.roll(now, 1, 0))
        two = pltpu.roll(now, 2, 0)
        two = jnp.where(row == 0, tail[14:15], jnp.where(row == 1, tail[15:16], two))
        conv = taps[0, layer : layer + 1] * two + taps[1, layer : layer + 1] * one + taps[2, layer : layer + 1] * now
        gat[layer, t] = (outer * conv).astype(bf16)

    def back(layer, b):
        span = pl.ds(b * rows, rows)
        total = xs[layer, t, span, :].astype(f32)
        depth = gat.shape[3]
        per = depth // wback.shape[2]
        for j in range(n_tp):
            w = wback[layer, per * j : per * (j + 1)].reshape(depth, feats)
            total = total + jnp.dot(gat[layer, j, span, :], w, preferred_element_type=f32)
        return total.astype(bf16)

    @pl.when(is_mid)
    def _():
        for u in range(min(4, units)):
            send_w(u, s, 0, opp, own=True)
        for u in range(units):
            pltpu.make_async_copy(own_w(u), held_w(u, s), sem_local.at[u]).start()
        @pl.when(outer_mid)
        def _():
            for j in range(n_tp):
                tok_partner(j).start()
        @pl.when(jnp.logical_not(outer_mid))
        def _():
            for j in range(n_tp):
                tok_local(j).start()
        for u in range(units):
            send_w(u, s, 1, partner, own=True)
        take_end(0)
        first = xs.at[0]
        @pl.when(outer_mid)
        def _():
            for b in range(2):
                place = xs.at[0, t, pl.ds(b * rows, rows)]
                remote(place, place, tok_send.at[b], tok_recv.at[b], partner, t).wait_recv()
            gather_start(0, first)
        pump(0)
        @pl.when(outer_mid)
        def _():
            gather_forward(0, first)
        pump(1)
        pump(2)
        @pl.when(outer_mid)
        def _():
            gather_near(0, first)
            gather_far(0, first)
        @pl.when(jnp.logical_not(outer_mid))
        def _():
            for j in range(n_tp):
                tok_local(j).wait()
                tok_partner(j).wait_recv()
        for layer in range(layers):
            for m in range(3):
                settle(4 * layer + m)
            x_g, gate_g = 2 * layer, 2 * layer + 1
            if layer == 0:
                for k, j in enumerate((t, tx, ty, td)):
                    project(layer, j, k == 0)
            else:
                project(layer, t, True)
                gather_near(x_g, xs.at[layer])
                project(layer, tx, False)
                project(layer, ty, False)
                gather_far(x_g, xs.at[layer])
                project(layer, td, False)
            gate(layer)
            g = gather_pieces(gate_g, gat.at[layer])
            g(t, 0, 0, tx).start()
            g(t, 0, 3, ty).start()
            g(t, 1, 1, ty).start()
            g(t, 1, 2, tx).start()
            pump(4 * layer + 3)
            g(tx, 0, 0, tx).wait_recv()
            g(tx, 0, 4, ty).start()
            g(ty, 1, 1, ty).wait_recv()
            g(ty, 1, 5, tx).start()
            settle(4 * layer + 3)

            def take_gated(b):
                if b == 0:
                    g(ty, 0, 3, ty).wait_recv()
                    g(td, 0, 4, ty).wait_recv()
                else:
                    g(tx, 1, 2, tx).wait_recv()
                    g(td, 1, 5, tx).wait_recv()

            if layer + 1 < layers:
                for b in range(2):
                    take_gated(b)
                    xs[layer + 1, t, b * rows : (b + 1) * rows, :] = back(layer, b)
                gather_start(x_g + 2, xs.at[layer + 1])
                pump(4 * layer + 4)
                gather_forward(x_g + 2, xs.at[layer + 1])
                pump(4 * layer + 5)
                pump(4 * layer + 6)
            else:
                for b in range(2):
                    mine = s == (n_sp // 2 - b)
                    take_gated(b)
                    res[b] = back(layer, b)
                    @pl.when(mine)
                    def _():
                        out[...] = res[b]
                    @pl.when(jnp.logical_not(mine))
                    def _():
                        result_copy(b).start()
        for u in range(units):
            for kind in range(6):
                remote(own_w(u), held_w(u, s), w_send.at[u, kind], w_recv.at[u, s], partner, t).wait_send()
        for layer in range(layers):
            if layer > 0:
                gather_drain(2 * layer, xs.at[layer])
            gather_drain(2 * layer + 1, gat.at[layer])
        @pl.when(outer_mid)
        def _():
            gather_drain(0, first)
            for j in range(n_tp):
                tok_partner(j).wait_send()
        @pl.when(s < n_sp - 3)
        def _():
            halo_copy(layers - 1).wait_send()
        for b in range(2):
            @pl.when(s != (n_sp // 2 - b))
            def _():
                result_copy(b).wait_send()
        @pl.when(outer_mid)
        def _():
            result_wait()


def fused(tokens, norm_gain, w_outer, w_inner, w_value, w_back, taps):
    n_sp, n_tp = lax.axis_size("sp"), lax.axis_size("tp")
    rows, width = tokens.shape
    layers, depth, chans = w_outer.shape
    back_rows, feats = w_back.shape[1:]
    dma = pltpu.SemaphoreType.DMA
    hbm, vmem = pl.BlockSpec(memory_space=pl.ANY), pl.BlockSpec(memory_space=pltpu.VMEM)
    return pl.pallas_call(
        mixer_kernel,
        out_shape=jax.ShapeDtypeStruct((rows, feats), bf16),
        in_specs=[hbm, vmem, hbm, hbm, hbm, hbm, vmem],
        out_specs=vmem,
        scratch_shapes=[
            pltpu.VMEM((layers, n_tp, 2 * rows, feats), bf16),
            pltpu.VMEM((3 * layers, n_sp, depth, chans), bf16),
            pltpu.VMEM((layers, n_sp, back_rows, feats), bf16),
            pltpu.VMEM((3, 2 * rows, chans), f32),
            pltpu.VMEM((2 * rows, 128), f32),
            pltpu.VMEM((layers, n_tp, 2 * rows, chans), bf16),
            pltpu.VMEM((2 * rows, chans), bf16),
            pltpu.VMEM((layers, 16, chans), bf16),
            pltpu.VMEM((2, rows, feats), bf16),
            pltpu.VMEM((rows, feats), bf16),
            dma((4 * layers,)),
            dma((n_tp,)),
            dma((n_tp,)),
            dma((n_tp,)),
            dma((4 * layers, 6)),
            dma((4 * layers, n_sp)),
            dma((2 * layers, 6)),
            dma((2 * layers, 6)),
            dma((layers,)),
            dma((layers,)),
            dma((2,)),
            dma,
        ],
        compiler_params=pltpu.CompilerParams(
            collective_id=0, has_side_effects=True, vmem_limit_bytes=60 * 1024 * 1024
        ),
        name="mixer",
    )(tokens, norm_gain, w_outer, w_inner, w_value, w_back, taps.transpose(1, 0, 2))


def solution(mesh):
    in_specs = (
        P("sp", None),
        P(),
        P(None, "sp", "tp"),
        P(None, "sp", "tp"),
        P(None, "sp", "tp"),
        P(None, "sp", "tp"),
        P(None, None, "tp"),
    )
    out_specs = P("sp", "tp")
    body = fused if (mesh.shape["sp"], mesh.shape["tp"]) == (8, 4) else per_device
    return jax.shard_map(
        body, mesh=mesh, in_specs=in_specs, out_specs=out_specs, check_vma=False
    )
```

profile of v0, /device:TPU:1, one launch (start us, length us, event | category | flops | bytes accessed | tf_op | source)
XLA Modules:
  0.0 138.2 jit_solution(8441976147457087312)
XLA Ops:
  0.0 136.3 %mixer.1 = bf16[256,1024]{1,0:T(8,128)(2,1)} custom-call(bf16[256,4096]{1,0:T(8,128)(2,1)} %tok.1, f32[2,4096]{1,0:T(2,128)} %gain.1, bf16[2,512,256]{2,1,0:T(8,128)(2,1)} %w_outer.1, bf16[2,512,256]{2,1,0:T(8,128)(2,1)} %w_inner.1, bf16[2,512,256]{2,1,0:T(8,128)(2,1)} %w_value.1, bf16[2,128,1024]{2,1,0:T(8,128)(2,1)} %w_back.1, f32[3,2,256]{2,1,0:T(2,128)} %bitcast.1), custom_call_target="tpu_custom_call" | custom-call | tf_op jit(solution)/shard_map/mixer/pallas_call | solution.py:415
  136.3 1.9 %copy.9 = bf16[256,1024]{1,0:T(8,128)(2,1)} copy(bf16[256,1024]{1,0:T(8,128)(2,1)} %mixer.1) | data formatting | bytes 1048576
where the time goes:
time: 139 us; the launch traced here: 138 us
  Pallas kernels  136 us (98%)
  local copies, waits for them, and re-layouts  1.87 us (1%)
    pallas_call x1, Pallas kernels, fused(): pl.pallas_call(mixer_kernel, out_shape=jax.ShapeDtypeStruct((rows, feats)...  136 us

commit v1 on v0

v1 whole, which is shorter than its diff:
```python
import functools

import jax
import jax.numpy as jnp
from jax import lax
from jax.experimental import pallas as pl
from jax.experimental.pallas import tpu as pltpu
from jax.sharding import PartitionSpec as P

MESH = pl.DeviceIdType.MESH
f32 = jnp.float32
bf16 = jnp.bfloat16

eps = 1e-06

OUTER, INNER, VALUE, BACK = 0, 1, 2, 3
FIRST = (INNER, VALUE, OUTER, BACK)
SECOND = tuple(4 + m for m in FIRST)
PIECES = (1, 1, 1, 2, 4, 2, 2, 4)
KINDS = 9


def shifted(block, axis, distance):
    devices = range(lax.axis_size(axis))
    route = [(i - distance, i) for i in devices if i - distance in devices]
    return lax.ppermute(block, axis, route)


def per_device(tokens, norm_gain, w_outer, w_inner, w_value, w_back, taps):
    layers = w_outer.shape[0]
    count = tokens.shape[0]
    feats = w_back.shape[2]
    own = lax.axis_index("tp")
    held = (
        lax.all_gather(w_outer, "sp", axis=1, tiled=True),
        lax.all_gather(w_inner, "sp", axis=1, tiled=True),
        lax.all_gather(w_value, "sp", axis=1, tiled=True),
        lax.all_gather(w_back, "sp", axis=1, tiled=True),
    )
    current = tokens
    resid = lax.dynamic_slice_in_dim(tokens, own * feats, feats, 1)
    for layer in range(layers):
        if layer > 0:
            current = lax.all_gather(resid, "tp", axis=1, tiled=True)
        xf = current.astype(jnp.float32)
        normed = (
            xf * lax.rsqrt(jnp.mean(xf * xf, axis=-1, keepdims=True) + eps) * norm_gain[layer]
        ).astype(jnp.bfloat16)
        outer = jnp.dot(normed, held[0][layer], preferred_element_type=jnp.float32)
        inner = jnp.dot(normed, held[1][layer], preferred_element_type=jnp.float32)
        value = jnp.dot(normed, held[2][layer], preferred_element_type=jnp.float32)
        outer = outer.astype(jnp.bfloat16)
        inner = inner.astype(jnp.bfloat16)
        value = value.astype(jnp.bfloat16)
        mixed = (inner.astype(jnp.float32) * value.astype(jnp.float32)).astype(jnp.bfloat16)
        before = shifted(mixed[count - 2 :], "sp", 1)
        padded = jnp.concatenate([before, mixed], axis=0).astype(jnp.float32)
        conv = (
            taps[layer, 0] * padded[:count]
            + taps[layer, 1] * padded[1 : count + 1]
            + taps[layer, 2] * padded[2:]
        )
        gated = (outer.astype(jnp.float32) * conv).astype(jnp.bfloat16)
        whole = lax.all_gather(gated, "tp", axis=1, tiled=True)
        proj = jnp.dot(whole, held[3][layer], preferred_element_type=jnp.float32)
        resid = (resid.astype(jnp.float32) + proj).astype(jnp.bfloat16)
    return resid


def first_chunk(u):
    return sum(PIECES[:u])


def mixer_kernel(
    tok, gain, w_outer, w_inner, w_value, w_back, taps, out,
    xr, x1, scl, win, wback, acc, bacc, ss, gat, gat_end, mixed, halo,
    sem_local, sem_tok, tok_send, tok_recv, w_send, w_recv,
    g_send, g_recv, h_send, h_recv, e_send, e_recv,
):
    s, t = lax.axis_index("sp"), lax.axis_index("tp")
    n_sp, n_tp = win.shape[1], xr.shape[1]
    rows, feats = xr.shape[2:]
    half = rows // 2
    width = feats * n_tp
    units = len(PIECES)
    core = lax.rem(s, 2)
    flip = 1 - 2 * core
    left = s < n_sp // 2
    side = jnp.where(left, 1, -1)
    plane = lax.div(s, 2)
    planes = n_sp // 2
    is_end = jnp.logical_or(plane == 0, plane == planes - 1)
    is_mid = jnp.logical_not(is_end)
    partner = s + flip
    near = jnp.where(is_mid, s - 2 * side, s + 2 * side)
    opp = jnp.where(is_mid, s + 2 * side, s + 4 * side)
    far = jnp.where(is_mid, s + 4 * side, s + 6 * side)
    tx = t + 1 - 2 * lax.rem(t, 2)
    ty = t + 2 - 4 * lax.div(t, 2)
    td = n_tp - 1 - t

    barrier = pltpu.get_barrier_semaphore()

    def greet(sp, tp):
        pl.semaphore_signal(barrier, inc=1, device_id=(sp, tp), device_id_type=MESH)

    greet(partner, t)
    greet(s, tx)
    greet(s, ty)
    greet(near, t)
    greet(near + flip, t)

    @pl.when(is_mid)
    def _():
        greet(opp, t)
        greet(opp + flip, t)
    pl.semaphore_wait(barrier, jnp.where(is_mid, 7, 5))

    projections = (w_outer, w_inner, w_value)

    def own_w(u):
        layer, m = u // 4, u % 4
        return projections[m].at[layer] if m < 3 else w_back.at[layer]

    def held_w(u, source):
        layer, m = u // 4, u % 4
        return win.at[3 * layer + m, source] if m < 3 else wback.at[layer, source]

    def remote(a, b, ssem, rsem, sp, tp):
        return pltpu.make_async_remote_copy(
            src_ref=a, dst_ref=b, send_sem=ssem, recv_sem=rsem, device_id=(sp, tp), device_id_type=MESH
        )

    def piece(ref, u, k):
        size = ref.shape[0] // PIECES[u]
        return ref.at[pl.ds(k * size, size)]

    def w_copy(u, k, source, kind, target, own=False):
        to = piece(held_w(u, source), u, k)
        a = piece(own_w(u), u, k) if own else to
        i = first_chunk(u) + k
        return remote(a, to, w_send.at[i, kind], w_recv.at[i, source], target, t)

    def send_own(u, kind, target):
        for k in range(PIECES[u]):
            w_copy(u, k, s, kind, target, own=True).start()

    def pieces_of(u):
        return range(PIECES[u])

    def relay_near(u, ks=None):
        for k in ks or pieces_of(u):
            w_copy(u, k, near, 3, partner).wait_recv()

            @pl.when(is_mid)
            def _():
                w_copy(u, k, near, 4, opp).start()
            w_copy(u, k, near, 3, partner).start()

    def relay_across(u, source, kind, ks=None):
        for k in ks or pieces_of(u):
            w_copy(u, k, source, kind, partner).wait_recv()
            if u >= 3:
                @pl.when(is_mid)
                def _():
                    w_copy(u, k, source, kind + 1, near).start()
            w_copy(u, k, source, kind, partner).start()

    def relay_opp(u, ks=None):
        relay_across(u, opp, 5, ks)

    def relay_far(u, ks=None):
        relay_across(u, far, 7, ks)

    def settle(u, source):
        for k in pieces_of(u):
            w_copy(u, k, source + flip, 1, partner).wait_recv()

    def local_w(u):
        return pltpu.make_async_copy(own_w(u), held_w(u, s), sem_local.at[u])

    def tok_cols(j):
        return tok.at[:, pl.ds(pl.multiple_of(j * feats, feats), feats)]

    def tok_local(j):
        return pltpu.make_async_copy(tok_cols(j), xr.at[1, j], sem_tok.at[j])

    def tok_part(h):
        cols = pl.ds(pl.multiple_of(t * feats, feats), feats)
        return remote(
            tok.at[pl.ds(h * half, half), cols], xr.at[0, t, pl.ds(h * half, half)],
            tok_send.at[h], tok_recv.at[h], near, t,
        )

    def end_part(h):
        return remote(
            gat_end.at[pl.ds(h * half, half)], gat.at[0, t, pl.ds(h * half, half)],
            e_send.at[h], e_recv.at[h], near, t,
        )

    class Gather:
        def __init__(self, g, buf):
            self.g, self.buf = g, buf

        def part(self, block, h, k, target):
            size = self.buf.shape[1] // 2
            ref = self.buf.at[block, pl.ds(h * size, size)]
            return remote(ref, ref, g_send.at[self.g, k], g_recv.at[self.g, k], s, target)

        def start(self, h):
            if h == 0:
                self.part(t, 0, 0, tx).start()
                self.part(t, 0, 3, ty).start()
            else:
                self.part(t, 1, 1, ty).start()
                self.part(t, 1, 2, tx).start()

        def start_all(self):
            self.part(t, 0, 0, tx).start()
            self.part(t, 1, 1, ty).start()
            self.part(t, 1, 2, tx).start()
            self.part(t, 0, 3, ty).start()

        def forward(self, h):
            if h == 0:
                self.part(tx, 0, 0, tx).wait_recv()
                self.part(tx, 0, 4, ty).start()
            else:
                self.part(ty, 1, 1, ty).wait_recv()
                self.part(ty, 1, 5, tx).start()

        def beside(self):
            self.part(tx, 1, 2, tx).wait_recv()
            self.part(ty, 0, 3, ty).wait_recv()

        def across(self):
            self.part(td, 0, 4, ty).wait_recv()
            self.part(td, 1, 5, tx).wait_recv()

        def drain(self):
            self.part(t, 0, 0, tx).wait_send()
            self.part(t, 1, 1, ty).wait_send()
            self.part(t, 1, 2, tx).wait_send()
            self.part(t, 0, 3, ty).wait_send()
            self.part(tx, 0, 4, ty).wait_send()
            self.part(ty, 1, 5, tx).wait_send()

    gather_tok = Gather(0, xr.at[0])
    gather_gat = (Gather(1, gat.at[0]), Gather(3, gat.at[1]))
    gather_x = Gather(2, x1)

    def scale(layer, source, b, j):
        step = 64

        def tile(r, carry):
            span = pl.ds(pl.multiple_of(r * step, step), step)
            x = source[j, span, :].astype(f32)
            sq = x * x
            part = sq[:, :128]
            for q in range(1, feats // 128):
                part = part + sq[:, 128 * q : 128 * (q + 1)]
            ss[b, span, :] += part
            cols = pl.ds(pl.multiple_of(j * feats, feats), feats)
            scl[b, j, span, :] = (x * gain[layer : layer + 1, cols]).astype(bf16)
            return carry

        lax.fori_loop(0, rows // step, tile, 0)

    def project(layer, m, sources, first):
        blocks = (0, 1) if layer == 0 else (0,)
        depth = win.shape[2]

        def tile(b, carry):
            total = None
            for source in sources:
                z = lax.div(source, 2)
                w = win[3 * layer + m, pl.ds(2 * z, 2)].reshape(2 * depth, win.shape[3])
                dot = jnp.dot(scl[b, z], w, preferred_element_type=f32)
                total = dot if total is None else total + dot
            if first:
                acc[m, b] = total
            else:
                acc[m, b] += total
            return carry

        if len(blocks) == 1:
            tile(0, 0)
        else:
            lax.fori_loop(0, len(blocks), tile, 0)

    def inv_of(b):
        return lax.rsqrt(jnp.sum(ss[b], axis=-1, keepdims=True) / width + eps)

    def mix(b, slot):
        inv = inv_of(b)
        inner = (acc[INNER, b] * inv).astype(bf16)
        value = (acc[VALUE, b] * inv).astype(bf16)
        mixed[slot] = (inner.astype(f32) * value.astype(f32)).astype(bf16)

    def convolve(layer, b, slot):
        now = mixed[slot].astype(f32)
        tail = halo[slot].astype(f32)
        row = lax.broadcasted_iota(jnp.int32, now.shape, 0)
        one = jnp.where(row == 0, tail[15:16], pltpu.roll(now, 1, 0))
        two = pltpu.roll(now, 2, 0)
        two = jnp.where(row == 0, tail[14:15], jnp.where(row == 1, tail[15:16], two))
        acc[VALUE, b] = taps[layer, 0:1] * two + taps[layer, 1:2] * one + taps[layer, 2:3] * now

    def gate(b):
        outer = (acc[OUTER, b] * inv_of(b)).astype(bf16).astype(f32)
        return (outer * acc[VALUE, b]).astype(bf16)

    def tail_copy(slot, to_slot, h, target):
        return remote(
            mixed.at[slot, pl.ds(rows - 16, 16)], halo.at[to_slot], h_send.at[slot], h_recv.at[h], target, t
        )

    def back_dot(layer, sources, cols):
        total = None
        for source in sources:
            z = lax.div(source, 2)
            w = wback[layer, pl.ds(2 * z, 2), :, cols].reshape(2 * wback.shape[2], cols.size)
            dot = jnp.dot(gat[layer, z], w, preferred_element_type=f32)
            total = dot if total is None else total + dot
        return total

    def by_columns(body):
        step = 256

        def tile(c, carry):
            body(pl.ds(pl.multiple_of(c * step, step), step))
            return carry

        lax.fori_loop(0, feats // step, tile, 0)

    @pl.when(is_mid)
    def _():
        for u in FIRST[:3]:
            send_own(u, 0, opp)
        for u in FIRST + SECOND:
            send_own(u, 1, partner)
        for u in FIRST[3:] + SECOND:
            send_own(u, 2, near)
        for j in range(n_tp):
            tok_local(j).start()
        for u in FIRST + SECOND:
            local_w(u).start()
        ss[...] = jnp.zeros(ss.shape, f32)
        for j in range(n_tp):
            tok_local(j).wait()

        def scale_own(j, carry):
            scale(0, xr.at[1], 1, j)
            return carry

        lax.fori_loop(0, n_tp, scale_own, 0)
        relay_near(INNER)
        send_own(BACK, 0, opp)
        relay_opp(INNER)
        for h in range(2):
            tok_part(h).wait_recv()
            gather_tok.start(h)
            relay_opp((VALUE, OUTER)[h])
        gather_tok.forward(0)
        relay_near(VALUE)
        relay_far(INNER)
        scale(0, xr.at[0], 0, t)
        gather_tok.forward(1)
        relay_near(OUTER)
        relay_opp(BACK)
        gather_tok.beside()
        scale(0, xr.at[0], 0, tx)
        scale(0, xr.at[0], 0, ty)
        gather_tok.across()
        scale(0, xr.at[0], 0, td)
        for u in FIRST[:3]:
            local_w(u).wait()
            settle(u, s)
            settle(u, near)
            settle(u, opp)
        settle(INNER, far)
        project(0, INNER, (s, near, opp, far), True)
        relay_near(BACK)
        for u in SECOND[:3]:
            send_own(u, 0, opp)
        project(0, OUTER, (s, near, opp), True)
        relay_far(VALUE)
        settle(VALUE, far)
        project(0, VALUE, (s, near, opp, far), True)
        for b in range(2):
            mix(b, b)

        @pl.when(core == 0)
        def _():
            for b in range(2):
                tail_copy(b, b, b, partner).start()

        @pl.when(jnp.logical_and(core == 1, left))
        def _():
            tail_copy(0, 1, 1, partner).start()
            tail_copy(1, 1, 1, s + 1).start()

        @pl.when(jnp.logical_and(core == 1, jnp.logical_not(left)))
        def _():
            tail_copy(1, 0, 0, partner).start()

        for b in range(2):
            if b == 0:
                start_of_all = s == 2

                @pl.when(start_of_all)
                def _():
                    halo[0] = jnp.zeros(halo.shape[1:], bf16)

                @pl.when(jnp.logical_not(start_of_all))
                def _():
                    tail_copy(0, 0, 0, partner).wait_recv()
            else:
                tail_copy(1, 1, 1, partner).wait_recv()
            convolve(0, b, b)
        relay_far(OUTER)
        settle(OUTER, far)
        project(0, OUTER, (far,), False)
        gat_end[...] = gate(0)
        for h in range(2):
            end_part(h).start()
        gat[0, t] = gate(1)
        gather_gat[0].start_all()
        relay_near(SECOND[0])
        gather_gat[0].forward(0)
        gather_gat[0].forward(1)
        relay_far(BACK)

    @pl.when(is_end)
    def _():
        send_own(INNER, 0, near)
        for h in range(2):
            tok_part(h).start()
        for u in FIRST[1:] + SECOND:
            send_own(u, 0, near)
        for u in FIRST[3:] + SECOND:
            send_own(u, 1, partner)
        tok_local(t).start()
        for u in FIRST[3:] + SECOND:
            local_w(u).start()
        tok_local(t).wait()
        for u in FIRST[3:] + SECOND:
            relay_near(u)
        relay_opp(BACK)
        for h in range(2):
            end_part(h).wait_recv()
            gather_gat[0].start(h)
        relay_far(BACK, (0,))
        gather_gat[0].forward(0)
        gather_gat[0].forward(1)
        relay_far(BACK, (1,))

    gather_gat[0].beside()
    gather_gat[0].across()
    local_w(BACK).wait()
    for source in (s, near, opp, far):
        settle(BACK, source)

    def finish_first(cols):
        total = xr[1, t, :, cols].astype(f32) + back_dot(0, (s, near, opp, far), cols)
        x1[t, :, cols] = total.astype(bf16)

    by_columns(finish_first)
    gather_x.start_all()

    @pl.when(is_mid)
    def _():
        relay_near(SECOND[1])
    relay_opp(SECOND[0])

    @pl.when(is_mid)
    def _():
        relay_near(SECOND[2])
        send_own(SECOND[3], 0, opp)
    ss[0] = jnp.zeros(ss.shape[1:], f32)
    scale(1, x1, 0, t)
    gather_x.forward(0)
    gather_x.forward(1)
    relay_opp(SECOND[1])

    @pl.when(is_mid)
    def _():
        relay_near(SECOND[3])
    gather_x.beside()
    scale(1, x1, 0, tx)
    scale(1, x1, 0, ty)
    relay_opp(SECOND[2])
    gather_x.across()
    scale(1, x1, 0, td)
    relay_far(SECOND[0])
    for u in SECOND[:3]:
        local_w(u).wait()
        settle(u, s)
        settle(u, near)
        settle(u, opp)
    for u in SECOND[:3]:
        project(1, u % 4, (s, near, opp), True)
    settle(SECOND[0], far)
    project(1, INNER, (far,), False)
    relay_far(SECOND[1])
    settle(SECOND[1], far)
    project(1, VALUE, (far,), False)

    @pl.when(is_mid)
    def _():
        @pl.when(core == 0)
        def _():
            for b in range(2):
                tail_copy(b, b, b, partner).wait_send()

        @pl.when(jnp.logical_and(core == 1, left))
        def _():
            tail_copy(0, 1, 1, partner).wait_send()
            tail_copy(1, 1, 1, s + 1).wait_send()

        @pl.when(jnp.logical_and(core == 1, jnp.logical_not(left)))
        def _():
            tail_copy(1, 0, 0, partner).wait_send()
    mix(0, 2)

    @pl.when(s < n_sp - 1)
    def _():
        tail_copy(2, 2, 2, s + 1).start()

    @pl.when(s == 0)
    def _():
        halo[2] = jnp.zeros(halo.shape[1:], bf16)

    @pl.when(s > 0)
    def _():
        tail_copy(2, 2, 2, partner).wait_recv()
    convolve(1, 0, 2)
    relay_far(SECOND[2])
    settle(SECOND[2], far)
    project(1, OUTER, (far,), False)
    gat[1, t] = gate(0)
    gather_gat[1].start_all()
    last = SECOND[3]
    relay_opp(last, (0, 1, 2))
    gather_gat[1].forward(0)
    gather_gat[1].forward(1)
    relay_opp(last, (3,))
    relay_far(last, (0,))
    gather_gat[1].beside()
    gather_gat[1].across()
    relay_far(last, (1,))
    local_w(last).wait()
    for source in (s, near, opp):
        settle(last, source)

    def start_last(cols):
        bacc[:, cols] = x1[t, :, cols].astype(f32) + back_dot(1, (s, near, opp), cols)

    by_columns(start_last)
    relay_far(last, (2, 3))
    settle(last, far)

    def finish_last(cols):
        out[:, cols] = (bacc[:, cols] + back_dot(1, (far,), cols)).astype(bf16)

    by_columns(finish_last)

    def sent(u, kind):
        for k in pieces_of(u):
            w_copy(u, k, s, kind, partner).wait_send()

    for u in range(units):
        if u >= 3:
            for kind in (0, 1, 3, 5, 7):
                sent(u, kind)

            @pl.when(is_mid)
            def _():
                for kind in (2, 4, 6, 8):
                    sent(u, kind)
        else:
            sent(u, 0)

            @pl.when(is_mid)
            def _():
                for kind in (1, 3, 4, 5, 7):
                    sent(u, kind)

    @pl.when(is_mid)
    def _():
        gather_tok.drain()
        for h in range(2):
            end_part(h).wait_send()

    @pl.when(is_end)
    def _():
        for h in range(2):
            tok_part(h).wait_send()
    gather_gat[0].drain()
    gather_x.drain()
    gather_gat[1].drain()

    @pl.when(s < n_sp - 1)
    def _():
        tail_copy(2, 2, 2, partner).wait_send()


def fused(tokens, norm_gain, w_outer, w_inner, w_value, w_back, taps):
    n_sp, n_tp = lax.axis_size("sp"), lax.axis_size("tp")
    rows, width = tokens.shape
    layers, depth, chans = w_outer.shape
    back_rows, feats = w_back.shape[1:]
    if 4 * layers != len(PIECES):
        return per_device(tokens, norm_gain, w_outer, w_inner, w_value, w_back, taps)
    chunks = sum(PIECES)
    dma = pltpu.SemaphoreType.DMA
    hbm, vmem = pl.BlockSpec(memory_space=pl.ANY), pl.BlockSpec(memory_space=pltpu.VMEM)
    return pl.pallas_call(
        mixer_kernel,
        out_shape=jax.ShapeDtypeStruct((rows, feats), bf16),
        in_specs=[hbm, vmem, hbm, hbm, hbm, hbm, vmem],
        out_specs=vmem,
        scratch_shapes=[
            pltpu.VMEM((2, n_tp, rows, feats), bf16),
            pltpu.VMEM((n_tp, rows, feats), bf16),
            pltpu.VMEM((2, n_tp, rows, feats), bf16),
            pltpu.VMEM((3 * layers, n_sp, depth, chans), bf16),
            pltpu.VMEM((layers, n_sp, back_rows, feats), bf16),
            pltpu.VMEM((3, 2, rows, chans), f32),
            pltpu.VMEM((rows, feats), f32),
            pltpu.VMEM((2, rows, 128), f32),
            pltpu.VMEM((layers, n_tp, rows, chans), bf16),
            pltpu.VMEM((rows, chans), bf16),
            pltpu.VMEM((3, rows, chans), bf16),
            pltpu.VMEM((3, 16, chans), bf16),
            dma((4 * layers,)),
            dma((n_tp,)),
            dma((2,)),
            dma((2,)),
            dma((chunks, KINDS)),
            dma((chunks, n_sp)),
            dma((4, 6)),
            dma((4, 6)),
            dma((3,)),
            dma((3,)),
            dma((2,)),
            dma((2,)),
        ],
        compiler_params=pltpu.CompilerParams(
            collective_id=0, has_side_effects=True, vmem_limit_bytes=60 * 1024 * 1024
        ),
        name="mixer",
    )(tokens, norm_gain, w_outer, w_inner, w_value, w_back, taps)


def solution(mesh):
    in_specs = (
        P("sp", None),
        P(),
        P(None, "sp", "tp"),
        P(None, "sp", "tp"),
        P(None, "sp", "tp"),
        P(None, "sp", "tp"),
        P(None, None, "tp"),
    )
    out_specs = P("sp", "tp")
    body = fused if (mesh.shape["sp"], mesh.shape["tp"]) == (8, 4) else per_device
    return jax.shard_map(
        body, mesh=mesh, in_specs=in_specs, out_specs=out_specs, check_vma=False
    )
```

time: 139 us -> 134 us (0.964)
  the two profiles are of different devices: /device:TPU:1 before, /device:TPU:25 now
where the time goes in v1:
time: 134 us
  Pallas kernels  131 us (98%)
  local copies, waits for them, and re-layouts  3.16 us (2%)
    pallas_call x1, Pallas kernels, fused(): pl.pallas_call(mixer_kernel, out_shape=jax.ShapeDtypeStruct((rows, feats)...  131 us
    unnamed x2, local copies, waits for them, and re-layouts  3.16 us

profile of v1, /device:TPU:25, one launch (start us, length us, event | category | flops | bytes accessed | tf_op | source)
XLA Modules:
  0.0 133.8 jit_solution(1249188707313030533)
XLA Ops:
  0.0 1.3 copy.8.taps
  1.3 130.7 %mixer.1 = bf16[256,1024]{1,0:T(8,128)(2,1)} custom-call(bf16[256,4096]{1,0:T(8,128)(2,1)} %tok.1, f32[2,4096]{1,0:T(2,128)} %gain.1, bf16[2,512,256]{2,1,0:T(8,128)(2,1)} %w_outer.1, bf16[2,512,256]{2,1,0:T(8,128)(2,1)} %w_inner.1, bf16[2,512,256]{2,1,0:T(8,128)(2,1)} %w_value.1, bf16[2,128,1024]{2,1,0:T(8,128)(2,1)} %w_back.1, f32[2,3,256]{2,1,0:T(4,128)} %copy.8.taps), custom_call_target="tpu_custom_call" | custom-call | tf_op jit(solution)/shard_map/mixer/pallas_call | solution.py:618
  132.0 1.9 %copy.10 = bf16[256,1024]{1,0:T(8,128)(2,1)} copy(bf16[256,1024]{1,0:T(8,128)(2,1)} %mixer.1) | data formatting | bytes 1048576

commit v2 on v1

--- a/solution.py
+++ b/solution.py
@@ -74,7 +74,7 @@
 def mixer_kernel(
     tok, gain, w_outer, w_inner, w_value, w_back, taps, out,
     xr, x1, scl, win, wback, acc, bacc, ss, gat, gat_end, mixed, halo,
-    sem_local, sem_tok, tok_send, tok_recv, w_send, w_recv,
+    sem_local, sem_tok, tok_send, tok_recv, w_send, w_recv, p_recv,
     g_send, g_recv, h_send, h_recv, e_send, e_recv,
 ):
     s, t = lax.axis_index("sp"), lax.axis_index("tp")
@@ -135,46 +135,69 @@
         size = ref.shape[0] // PIECES[u]
         return ref.at[pl.ds(k * size, size)]
 
-    def w_copy(u, k, source, kind, target, own=False):
-        to = piece(held_w(u, source), u, k)
-        a = piece(own_w(u), u, k) if own else to
-        i = first_chunk(u) + k
-        return remote(a, to, w_send.at[i, kind], w_recv.at[i, source], target, t)
-
-    def send_own(u, kind, target):
-        for k in range(PIECES[u]):
-            w_copy(u, k, s, kind, target, own=True).start()
+    OWN, NEAR, OPP, FAR = 0, 1, 2, 3
+    source_of = (s, near, opp, far)
+
+    def w_copy(u, k, role, kind, to_role, target):
+        to = piece(held_w(u, source_of[role]), u, k)
+        a = piece(own_w(u), u, k) if role == OWN else to
+        return remote(a, to, w_send.at[kind], w_recv.at[first_chunk(u) + k, to_role - 1], target, t)
+
+    def to_partner(u, k, role):
+        to = piece(held_w(u, source_of[role]), u, k)
+        a = piece(own_w(u), u, k) if role == OWN else to
+        return remote(a, to, w_send.at[role], p_recv.at[u, role], partner, t)
 
     def pieces_of(u):
         return range(PIECES[u])
 
+    def arrived(u, k, role):
+        to = piece(held_w(u, source_of[role]), u, k)
+        remote(to, to, w_send.at[0], w_recv.at[first_chunk(u) + k, role - 1], partner, t).wait_recv()
+
+    def send_opp(u):
+        for k in pieces_of(u):
+            w_copy(u, k, OWN, 4, OPP, opp).start()
+
+    def send_near(u):
+        for k in pieces_of(u):
+            w_copy(u, k, OWN, 5, NEAR, near).start()
+
+    def send_partner(u):
+        for k in pieces_of(u):
+            to_partner(u, k, OWN).start()
+
     def relay_near(u, ks=None):
         for k in ks or pieces_of(u):
-            w_copy(u, k, near, 3, partner).wait_recv()
+            arrived(u, k, NEAR)
 
             @pl.when(is_mid)
             def _():
-                w_copy(u, k, near, 4, opp).start()
-            w_copy(u, k, near, 3, partner).start()
-
-    def relay_across(u, source, kind, ks=None):
+                w_copy(u, k, NEAR, 6, FAR, opp).start()
+            to_partner(u, k, NEAR).start()
+
+    def relay_across(u, role, ks=None):
         for k in ks or pieces_of(u):
-            w_copy(u, k, source, kind, partner).wait_recv()
+            arrived(u, k, role)
             if u >= 3:
                 @pl.when(is_mid)
                 def _():
-                    w_copy(u, k, source, kind + 1, near).start()
-            w_copy(u, k, source, kind, partner).start()
+                    w_copy(u, k, role, 5 + role, role, near).start()
+            to_partner(u, k, role).start()
 
     def relay_opp(u, ks=None):
-        relay_across(u, opp, 5, ks)
+        relay_across(u, OPP, ks)
 
     def relay_far(u, ks=None):
-        relay_across(u, far, 7, ks)
-
-    def settle(u, source):
-        for k in pieces_of(u):
-            w_copy(u, k, source + flip, 1, partner).wait_recv()
+        relay_across(u, FAR, ks)
+
+    def settle(u, role):
+        to = held_w(u, source_of[role] + flip)
+        remote(to, to, w_send.at[0], p_recv.at[u, role], partner, t).wait_recv()
+
+    def sent(kind, count):
+        ref = win.at[0, pl.ds(0, count)]
+        remote(ref, ref, w_send.at[kind], p_recv.at[0, 0], partner, t).wait_send()
 
     def local_w(u):
         return pltpu.make_async_copy(own_w(u), held_w(u, s), sem_local.at[u])
@@ -205,7 +228,12 @@
         def part(self, block, h, k, target):
             size = self.buf.shape[1] // 2
             ref = self.buf.at[block, pl.ds(h * size, size)]
-            return remote(ref, ref, g_send.at[self.g, k], g_recv.at[self.g, k], s, target)
+            slot = (0, 1, 2, 2, 3, 3)[k]
+            return remote(ref, ref, g_send.at[self.g], g_recv.at[self.g, slot], s, target)
+
+        def whole(self, blocks, slot):
+            ref = self.buf.at[pl.ds(0, blocks)]
+            return remote(ref, ref, g_send.at[self.g], g_recv.at[self.g, slot], s, tx)
 
         def start(self, h):
             if h == 0:
@@ -230,20 +258,13 @@
                 self.part(ty, 1, 5, tx).start()
 
         def beside(self):
-            self.part(tx, 1, 2, tx).wait_recv()
-            self.part(ty, 0, 3, ty).wait_recv()
+            self.whole(1, 2).wait_recv()
 
         def across(self):
-            self.part(td, 0, 4, ty).wait_recv()
-            self.part(td, 1, 5, tx).wait_recv()
+            self.whole(1, 3).wait_recv()
 
         def drain(self):
-            self.part(t, 0, 0, tx).wait_send()
-            self.part(t, 1, 1, ty).wait_send()
-            self.part(t, 1, 2, tx).wait_send()
-            self.part(t, 0, 3, ty).wait_send()
-            self.part(tx, 0, 4, ty).wait_send()
-            self.part(ty, 1, 5, tx).wait_send()
+            self.whole(3, 0).wait_send()
 
     gather_tok = Gather(0, xr.at[0])
     gather_gat = (Gather(1, gat.at[0]), Gather(3, gat.at[1]))
@@ -272,8 +293,8 @@
 
         def tile(b, carry):
             total = None
-            for source in sources:
-                z = lax.div(source, 2)
+            for role in sources:
+                z = lax.div(source_of[role], 2)
                 w = win[3 * layer + m, pl.ds(2 * z, 2)].reshape(2 * depth, win.shape[3])
                 dot = jnp.dot(scl[b, z], w, preferred_element_type=f32)
                 total = dot if total is None else total + dot
@@ -304,7 +325,7 @@
         one = jnp.where(row == 0, tail[15:16], pltpu.roll(now, 1, 0))
         two = pltpu.roll(now, 2, 0)
         two = jnp.where(row == 0, tail[14:15], jnp.where(row == 1, tail[15:16], two))
-        acc[VALUE, b] = taps[layer, 0:1] * two + taps[layer, 1:2] * one + taps[layer, 2:3] * now
+        acc[VALUE, b] = taps[0, layer : layer + 1] * two + taps[1, layer : layer + 1] * one + taps[2, layer : layer + 1] * now
 
     def gate(b):
         outer = (acc[OUTER, b] * inv_of(b)).astype(bf16).astype(f32)
@@ -317,8 +338,8 @@
 
     def back_dot(layer, sources, cols):
         total = None
-        for source in sources:
-            z = lax.div(source, 2)
+        for role in sources:
+            z = lax.div(source_of[role], 2)
             w = wback[layer, pl.ds(2 * z, 2), :, cols].reshape(2 * wback.shape[2], cols.size)
             dot = jnp.dot(gat[layer, z], w, preferred_element_type=f32)
             total = dot if total is None else total + dot
@@ -336,11 +357,11 @@
     @pl.when(is_mid)
     def _():
         for u in FIRST[:3]:
-            send_own(u, 0, opp)
+            send_opp(u)
         for u in FIRST + SECOND:
-            send_own(u, 1, partner)
+            send_partner(u)
         for u in FIRST[3:] + SECOND:
-            send_own(u, 2, near)
+            send_near(u)
         for j in range(n_tp):
             tok_local(j).start()
         for u in FIRST + SECOND:
@@ -355,7 +376,7 @@
 
         lax.fori_loop(0, n_tp, scale_own, 0)
         relay_near(INNER)
-        send_own(BACK, 0, opp)
+        send_opp(BACK)
         relay_opp(INNER)
         for h in range(2):
             tok_part(h).wait_recv()
@@ -375,18 +396,14 @@
         scale(0, xr.at[0], 0, td)
         for u in FIRST[:3]:
             local_w(u).wait()
-            settle(u, s)
-            settle(u, near)
-            settle(u, opp)
-        settle(INNER, far)
-        project(0, INNER, (s, near, opp, far), True)
-        relay_near(BACK)
-        for u in SECOND[:3]:
-            send_own(u, 0, opp)
-        project(0, OUTER, (s, near, opp), True)
+            for role in (OWN, NEAR, OPP):
+                settle(u, role)
+        settle(INNER, FAR)
+        project(0, INNER, (OWN, NEAR, OPP, FAR), True)
+        project(0, VALUE, (OWN, NEAR, OPP), True)
         relay_far(VALUE)
-        settle(VALUE, far)
-        project(0, VALUE, (s, near, opp, far), True)
+        settle(VALUE, FAR)
+        project(0, VALUE, (FAR,), False)
         for b in range(2):
             mix(b, b)
 
@@ -397,13 +414,17 @@
 
         @pl.when(jnp.logical_and(core == 1, left))
         def _():
+            tail_copy(1, 1, 1, s + 1).start()
             tail_copy(0, 1, 1, partner).start()
-            tail_copy(1, 1, 1, s + 1).start()
 
         @pl.when(jnp.logical_and(core == 1, jnp.logical_not(left)))
         def _():
             tail_copy(1, 0, 0, partner).start()
-
+        relay_near(BACK)
+        for u in SECOND[:3]:
+            send_opp(u)
+        project(0, OUTER, (OWN, NEAR, OPP), True)
+        relay_far(OUTER)
         for b in range(2):
             if b == 0:
                 start_of_all = s == 2
@@ -418,9 +439,8 @@
             else:
                 tail_copy(1, 1, 1, partner).wait_recv()
             convolve(0, b, b)
-        relay_far(OUTER)
-        settle(OUTER, far)
-        project(0, OUTER, (far,), False)
+        settle(OUTER, FAR)
+        project(0, OUTER, (FAR,), False)
         gat_end[...] = gate(0)
         for h in range(2):
             end_part(h).start()
@@ -433,13 +453,13 @@
 
     @pl.when(is_end)
     def _():
-        send_own(INNER, 0, near)
+        send_near(INNER)
         for h in range(2):
             tok_part(h).start()
         for u in FIRST[1:] + SECOND:
-            send_own(u, 0, near)
+            send_near(u)
         for u in FIRST[3:] + SECOND:
-            send_own(u, 1, partner)
+            send_partner(u)
         tok_local(t).start()
         for u in FIRST[3:] + SECOND:
             local_w(u).start()
@@ -458,11 +478,11 @@
     gather_gat[0].beside()
     gather_gat[0].across()
     local_w(BACK).wait()
-    for source in (s, near, opp, far):
-        settle(BACK, source)
+    for role in (OWN, NEAR, OPP, FAR):
+        settle(BACK, role)
 
     def finish_first(cols):
-        total = xr[1, t, :, cols].astype(f32) + back_dot(0, (s, near, opp, far), cols)
+        total = xr[1, t, :, cols].astype(f32) + back_dot(0, (OWN, NEAR, OPP, FAR), cols)
         x1[t, :, cols] = total.astype(bf16)
 
     by_columns(finish_first)
@@ -476,16 +496,11 @@
     @pl.when(is_mid)
     def _():
         relay_near(SECOND[2])
-        send_own(SECOND[3], 0, opp)
     ss[0] = jnp.zeros(ss.shape[1:], f32)
     scale(1, x1, 0, t)
     gather_x.forward(0)
     gather_x.forward(1)
     relay_opp(SECOND[1])
-
-    @pl.when(is_mid)
-    def _():
-        relay_near(SECOND[3])
     gather_x.beside()
     scale(1, x1, 0, tx)
     scale(1, x1, 0, ty)
@@ -495,37 +510,31 @@
     relay_far(SECOND[0])
     for u in SECOND[:3]:
         local_w(u).wait()
-        settle(u, s)
-        settle(u, near)
-        settle(u, opp)
+        for role in (OWN, NEAR, OPP):
+            settle(u, role)
     for u in SECOND[:3]:
-        project(1, u % 4, (s, near, opp), True)
-    settle(SECOND[0], far)
-    project(1, INNER, (far,), False)
+        project(1, u % 4, (OWN, NEAR, OPP), True)
+    settle(SECOND[0], FAR)
+    project(1, INNER, (FAR,), False)
     relay_far(SECOND[1])
-    settle(SECOND[1], far)
-    project(1, VALUE, (far,), False)
+    settle(SECOND[1], FAR)
+    project(1, VALUE, (FAR,), False)
+    mix(0, 2)
+
+    @pl.when(s < n_sp - 1)
+    def _():
+        tail_copy(2, 2, 2, s + 1).start()
+    last = SECOND[3]
 
     @pl.when(is_mid)
     def _():
-        @pl.when(core == 0)
-        def _():
-            for b in range(2):
-                tail_copy(b, b, b, partner).wait_send()
-
-        @pl.when(jnp.logical_and(core == 1, left))
-        def _():
-            tail_copy(0, 1, 1, partner).wait_send()
-            tail_copy(1, 1, 1, s + 1).wait_send()
-
-        @pl.when(jnp.logical_and(core == 1, jnp.logical_not(left)))
-        def _():
-            tail_copy(1, 0, 0, partner).wait_send()
-    mix(0, 2)
-
-    @pl.when(s < n_sp - 1)
-    def _():
-        tail_copy(2, 2, 2, s + 1).start()
+        send_opp(last)
+        relay_near(last)
+    relay_far(SECOND[2])
+
+    @pl.when(is_mid)
+    def _():
+        relay_opp(last, (0, 1))
 
     @pl.when(s == 0)
     def _():
@@ -535,65 +544,68 @@
     def _():
         tail_copy(2, 2, 2, partner).wait_recv()
     convolve(1, 0, 2)
-    relay_far(SECOND[2])
-    settle(SECOND[2], far)
-    project(1, OUTER, (far,), False)
+    settle(SECOND[2], FAR)
+    project(1, OUTER, (FAR,), False)
     gat[1, t] = gate(0)
     gather_gat[1].start_all()
-    last = SECOND[3]
-    relay_opp(last, (0, 1, 2))
+
+    @pl.when(is_end)
+    def _():
+        relay_opp(last, (0, 1))
+    relay_opp(last, (2, 3))
     gather_gat[1].forward(0)
     gather_gat[1].forward(1)
-    relay_opp(last, (3,))
     relay_far(last, (0,))
     gather_gat[1].beside()
     gather_gat[1].across()
     relay_far(last, (1,))
     local_w(last).wait()
-    for source in (s, near, opp):
-        settle(last, source)
+    for role in (OWN, NEAR, OPP):
+        settle(last, role)
 
     def start_last(cols):
-        bacc[:, cols] = x1[t, :, cols].astype(f32) + back_dot(1, (s, near, opp), cols)
+        bacc[:, cols] = x1[t, :, cols].astype(f32) + back_dot(1, (OWN, NEAR, OPP), cols)
 
     by_columns(start_last)
     relay_far(last, (2, 3))
-    settle(last, far)
+    settle(last, FAR)
 
     def finish_last(cols):
-        out[:, cols] = (bacc[:, cols] + back_dot(1, (far,), cols)).astype(bf16)
+        out[:, cols] = (bacc[:, cols] + back_dot(1, (FAR,), cols)).astype(bf16)
 
     by_columns(finish_last)
 
-    def sent(u, kind):
-        for k in pieces_of(u):
-            w_copy(u, k, s, kind, partner).wait_send()
-
-    for u in range(units):
-        if u >= 3:
-            for kind in (0, 1, 3, 5, 7):
-                sent(u, kind)
-
-            @pl.when(is_mid)
-            def _():
-                for kind in (2, 4, 6, 8):
-                    sent(u, kind)
-        else:
-            sent(u, 0)
-
-            @pl.when(is_mid)
-            def _():
-                for kind in (1, 3, 4, 5, 7):
-                    sent(u, kind)
+    some = units - 3
 
     @pl.when(is_mid)
     def _():
+        for kind in (0, 1, 2, 3, 4, 6):
+            sent(kind, units)
+        for kind in (5, 7, 8):
+            sent(kind, some)
         gather_tok.drain()
         for h in range(2):
             end_part(h).wait_send()
 
+        @pl.when(core == 0)
+        def _():
+            for b in range(2):
+                tail_copy(b, b, b, partner).wait_send()
+
+        @pl.when(jnp.logical_and(core == 1, left))
+        def _():
+            tail_copy(0, 1, 1, partner).wait_send()
+            tail_copy(1, 1, 1, s + 1).wait_send()
+
+        @pl.when(jnp.logical_and(core == 1, jnp.logical_not(left)))
+        def _():
+            tail_copy(1, 0, 0, partner).wait_send()
+
     @pl.when(is_end)
     def _():
+        for kind in (0, 1, 2, 3):
+            sent(kind, some)
+        sent(5, units)
         for h in range(2):
             tok_part(h).wait_send()
     gather_gat[0].drain()
@@ -637,10 +649,11 @@
             dma((n_tp,)),
             dma((2,)),
             dma((2,)),
-            dma((chunks, KINDS)),
-            dma((chunks, n_sp)),
-            dma((4, 6)),
-            dma((4, 6)),
+            dma((KINDS,)),
+            dma((chunks, 3)),
+            dma((4 * layers, 4)),
+            dma((4,)),
+            dma((4, 4)),
             dma((3,)),
             dma((3,)),
             dma((2,)),
@@ -650,7 +663,7 @@
             collective_id=0, has_side_effects=True, vmem_limit_bytes=60 * 1024 * 1024
         ),
         name="mixer",
-    )(tokens, norm_gain, w_outer, w_inner, w_value, w_back, taps)
+    )(tokens, norm_gain, w_outer, w_inner, w_value, w_back, taps.transpose(1, 0, 2))
 
 
 def solution(mesh):

time: 134 us -> 112 us (0.84)
  the two profiles are of different devices: /device:TPU:25 before, /device:TPU:1 now
where the time goes in v2:
time: 112 us
  Pallas kernels  110 us (98%)
  local copies, waits for them, and re-layouts  1.87 us (2%)
    pallas_call x1, Pallas kernels, fused(): pl.pallas_call(mixer_kernel, out_shape=jax.ShapeDtypeStruct((rows, feats)...  110 us

profile of v2, /device:TPU:1, one launch (start us, length us, event | category | flops | bytes accessed | tf_op | source)
XLA Modules:
  0.0 111.9 jit_solution(3966664105335870889)
XLA Ops:
  0.0 110.0 %mixer.1 = bf16[256,1024]{1,0:T(8,128)(2,1)} custom-call(bf16[256,4096]{1,0:T(8,128)(2,1)} %tok.1, f32[2,4096]{1,0:T(2,128)} %gain.1, bf16[2,512,256]{2,1,0:T(8,128)(2,1)} %w_outer.1, bf16[2,512,256]{2,1,0:T(8,128)(2,1)} %w_inner.1, bf16[2,512,256]{2,1,0:T(8,128)(2,1)} %w_value.1, bf16[2,128,1024]{2,1,0:T(8,128)(2,1)} %w_back.1, f32[3,2,256]{2,1,0:T(2,128)} %bitcast.1), custom_call_target="tpu_custom_call" | custom-call | tf_op jit(solution)/shard_map/mixer/pallas_call | solution.py:630
  110.0 1.9 %copy.9 = bf16[256,1024]{1,0:T(8,128)(2,1)} copy(bf16[256,1024]{1,0:T(8,128)(2,1)} %mixer.1) | data formatting | bytes 1048576

commit v3 on v2

--- a/solution.py
+++ b/solution.py
@@ -498,16 +498,16 @@
         relay_near(SECOND[2])
     ss[0] = jnp.zeros(ss.shape[1:], f32)
     scale(1, x1, 0, t)
+    relay_opp(SECOND[1])
     gather_x.forward(0)
     gather_x.forward(1)
-    relay_opp(SECOND[1])
+    relay_opp(SECOND[2])
     gather_x.beside()
     scale(1, x1, 0, tx)
     scale(1, x1, 0, ty)
-    relay_opp(SECOND[2])
+    relay_far(SECOND[0])
     gather_x.across()
     scale(1, x1, 0, td)
-    relay_far(SECOND[0])
     for u in SECOND[:3]:
         local_w(u).wait()
         for role in (OWN, NEAR, OPP):
@@ -534,7 +534,7 @@
 
     @pl.when(is_mid)
     def _():
-        relay_opp(last, (0, 1))
+        relay_opp(last)
 
     @pl.when(s == 0)
     def _():
@@ -551,14 +551,19 @@
 
     @pl.when(is_end)
     def _():
-        relay_opp(last, (0, 1))
-    relay_opp(last, (2, 3))
+        relay_opp(last)
+
+    @pl.when(is_mid)
+    def _():
+        relay_far(last, (0, 1))
     gather_gat[1].forward(0)
     gather_gat[1].forward(1)
-    relay_far(last, (0,))
+
+    @pl.when(is_mid)
+    def _():
+        relay_far(last, (2, 3))
     gather_gat[1].beside()
     gather_gat[1].across()
-    relay_far(last, (1,))
     local_w(last).wait()
     for role in (OWN, NEAR, OPP):
         settle(last, role)
@@ -567,7 +572,10 @@
         bacc[:, cols] = x1[t, :, cols].astype(f32) + back_dot(1, (OWN, NEAR, OPP), cols)
 
     by_columns(start_last)
-    relay_far(last, (2, 3))
+
+    @pl.when(is_end)
+    def _():
+        relay_far(last)
     settle(last, FAR)
 
     def finish_last(cols):

time: 112 us -> 111 us (level)
  Pallas kernels: 110 us -> 108 us
    pallas_call x1, Pallas kernels: 110 us -> 108 us  [fused(): pl.pallas_call(mixer_kernel, out_shape=jax.ShapeDtypeStruct((rows, feats)...]
where the time goes in v3:
time: 111 us; the launch traced here: 110 us
  Pallas kernels  108 us (97%)
  local copies, waits for them, and re-layouts  1.87 us (2%)
    pallas_call x1, Pallas kernels, fused(): pl.pallas_call(mixer_kernel, out_shape=jax.ShapeDtypeStruct((rows, feats)...  108 us

profile of v3, /device:TPU:1, one launch (start us, length us, event | category | flops | bytes accessed | tf_op | source)
XLA Modules:
  0.0 109.9 jit_solution(17886613557465077571)
XLA Ops:
  0.0 108.1 %mixer.1 = bf16[256,1024]{1,0:T(8,128)(2,1)} custom-call(bf16[256,4096]{1,0:T(8,128)(2,1)} %tok.1, f32[2,4096]{1,0:T(2,128)} %gain.1, bf16[2,512,256]{2,1,0:T(8,128)(2,1)} %w_outer.1, bf16[2,512,256]{2,1,0:T(8,128)(2,1)} %w_inner.1, bf16[2,512,256]{2,1,0:T(8,128)(2,1)} %w_value.1, bf16[2,128,1024]{2,1,0:T(8,128)(2,1)} %w_back.1, f32[3,2,256]{2,1,0:T(2,128)} %bitcast.1), custom_call_target="tpu_custom_call" | custom-call | tf_op jit(solution)/shard_map/mixer/pallas_call | solution.py:638
  108.1 1.9 %copy.9 = bf16[256,1024]{1,0:T(8,128)(2,1)} copy(bf16[256,1024]{1,0:T(8,128)(2,1)} %mixer.1) | data formatting | bytes 1048576

commit v4 on v3

--- a/solution.py
+++ b/solution.py
@@ -72,9 +72,9 @@
 
 
 def mixer_kernel(
-    tok, gain, w_outer, w_inner, w_value, w_back, taps, out,
-    xr, x1, scl, win, wback, acc, bacc, ss, gat, gat_end, mixed, halo,
-    sem_local, sem_tok, tok_send, tok_recv, w_send, w_recv, p_recv,
+    tok, gain_hbm, w_outer, w_inner, w_value, w_back, taps_hbm, out,
+    gain, taps, xr, x1, scl, win, wback, acc, bacc, ss, gat, gat_end, mixed, halo,
+    sem_small, sem_local, sem_tok, tok_send, tok_recv, w_send, w_recv, p_recv,
     g_send, g_recv, h_send, h_recv, e_send, e_recv,
 ):
     s, t = lax.axis_index("sp"), lax.axis_index("tp")
@@ -99,6 +99,12 @@
     ty = t + 2 - 4 * lax.div(t, 2)
     td = n_tp - 1 - t
 
+    small = (
+        pltpu.make_async_copy(gain_hbm, gain, sem_small.at[0]),
+        pltpu.make_async_copy(taps_hbm, taps, sem_small.at[1]),
+    )
+    for copy in small:
+        copy.start()
     barrier = pltpu.get_barrier_semaphore()
 
     def greet(sp, tp):
@@ -115,6 +121,8 @@
         greet(opp, t)
         greet(opp + flip, t)
     pl.semaphore_wait(barrier, jnp.where(is_mid, 7, 5))
+    for copy in small:
+        copy.wait()
 
     projections = (w_outer, w_inner, w_value)
 
@@ -635,12 +643,18 @@
     chunks = sum(PIECES)
     dma = pltpu.SemaphoreType.DMA
     hbm, vmem = pl.BlockSpec(memory_space=pl.ANY), pl.BlockSpec(memory_space=pltpu.VMEM)
+    held = [
+        pltpu.with_memory_space_constraint(a, pltpu.HBM)
+        for a in (tokens, norm_gain, w_outer, w_inner, w_value, w_back, taps.transpose(1, 0, 2))
+    ]
     return pl.pallas_call(
         mixer_kernel,
         out_shape=jax.ShapeDtypeStruct((rows, feats), bf16),
-        in_specs=[hbm, vmem, hbm, hbm, hbm, hbm, vmem],
+        in_specs=[hbm] * 7,
         out_specs=vmem,
         scratch_shapes=[
+            pltpu.VMEM((layers, width), f32),
+            pltpu.VMEM(taps.shape[1:2] + taps.shape[:1] + taps.shape[2:], f32),
             pltpu.VMEM((2, n_tp, rows, feats), bf16),
             pltpu.VMEM((n_tp, rows, feats), bf16),
             pltpu.VMEM((2, n_tp, rows, feats), bf16),
@@ -653,6 +667,7 @@
             pltpu.VMEM((rows, chans), bf16),
             pltpu.VMEM((3, rows, chans), bf16),
             pltpu.VMEM((3, 16, chans), bf16),
+            dma((2,)),
             dma((4 * layers,)),
             dma((n_tp,)),
             dma((2,)),
@@ -668,10 +683,10 @@
             dma((2,)),
         ],
         compiler_params=pltpu.CompilerParams(
-            collective_id=0, has_side_effects=True, vmem_limit_bytes=60 * 1024 * 1024
+            collective_id=0, has_side_effects=True, vmem_limit_bytes=48 * 1024 * 1024
         ),
         name="mixer",
-    )(tokens, norm_gain, w_outer, w_inner, w_value, w_back, taps.transpose(1, 0, 2))
+    )(*held)
 
 
 def solution(mesh):

time: 111 us -> 108 us (0.973)
    pallas_call x1, Pallas kernels: 108 us -> 107 us  [fused(): pl.pallas_call(mixer_kernel, out_shape=jax.ShapeDtypeStruct((rows, feats)...]
where the time goes in v4:
time: 108 us; the launch traced here: 107 us
  Pallas kernels  107 us (99%)
    pallas_call x1, Pallas kernels, fused(): pl.pallas_call(mixer_kernel, out_shape=jax.ShapeDtypeStruct((rows, feats)...  107 us

profile of v4, /device:TPU:1, one launch (start us, length us, event | category | flops | bytes accessed | tf_op | source)
XLA Modules:
  0.0 107.3 jit_solution(14481321454672029832)
XLA Ops:
  0.0 106.5 %mixer.1 = bf16[256,1024]{1,0:T(8,128)(2,1)S(1)} custom-call(bf16[256,4096]{1,0:T(8,128)(2,1)} %tok.1, f32[2,4096]{1,0:T(2,128)} %gain_hbm.1, bf16[2,512,256]{2,1,0:T(8,128)(2,1)} %w_outer.1, bf16[2,512,256]{2,1,0:T(8,128)(2,1)} %w_inner.1, bf16[2,512,256]{2,1,0:T(8,128)(2,1)} %w_value.1, bf16[2,128,1024]{2,1,0:T(8,128)(2,1)} %w_back.1, f32[3,2,256]{2,1,0:T(2,128)} %bitcast.1), custom_call_target="tpu_custom_call" | custom-call | tf_op jit(solution)/shard_map/mixer/pallas_call | solution.py:650
  106.5 0.8 copy.9

commit v5 on v4

--- a/solution.py
+++ b/solution.py
@@ -14,8 +14,9 @@
 eps = 1e-06
 
 OUTER, INNER, VALUE, BACK = 0, 1, 2, 3
-FIRST = (INNER, VALUE, OUTER, BACK)
-SECOND = tuple(4 + m for m in FIRST)
+FIRST = (INNER, VALUE, OUTER)
+SECOND = tuple(4 + m for m in FIRST + (BACK,))
+SHARED = (BACK,) + SECOND
 PIECES = (1, 1, 1, 2, 4, 2, 2, 4)
 KINDS = 9
 
@@ -73,13 +74,14 @@
 
 def mixer_kernel(
     tok, gain_hbm, w_outer, w_inner, w_value, w_back, taps_hbm, out,
-    gain, taps, xr, x1, scl, win, wback, acc, bacc, ss, gat, gat_end, mixed, halo,
-    sem_small, sem_local, sem_tok, tok_send, tok_recv, w_send, w_recv, p_recv,
+    gain, taps, xr, xq, stage, x1, scl, sclh, cbuf, cin, win, wback, acc, bacc, ss, gat, gat_end, mixed, halo,
+    sem_small, sem_local, sem_tok, t_send, t_recv, c_send, c_recv, s_send, s_recv, w_send, w_recv, p_recv,
     g_send, g_recv, h_send, h_recv, e_send, e_recv,
 ):
     s, t = lax.axis_index("sp"), lax.axis_index("tp")
-    n_sp, n_tp = win.shape[1], xr.shape[1]
-    rows, feats = xr.shape[2:]
+    n_sp, n_tp = win.shape[1], xr.shape[0]
+    rows, feats = xr.shape[1:]
+    quarter = xq.shape[3]
     half = rows // 2
     width = feats * n_tp
     units = len(PIECES)
@@ -87,6 +89,7 @@
     flip = 1 - 2 * core
     left = s < n_sp // 2
     side = jnp.where(left, 1, -1)
+    own_half = jnp.where(left, 0, 1)
     plane = lax.div(s, 2)
     planes = n_sp // 2
     is_end = jnp.logical_or(plane == 0, plane == planes - 1)
@@ -179,18 +182,19 @@
         for k in ks or pieces_of(u):
             arrived(u, k, NEAR)
 
-            @pl.when(is_mid)
-            def _():
-                w_copy(u, k, NEAR, 6, FAR, opp).start()
+            if u >= 3:
+                @pl.when(is_mid)
+                def _():
+                    w_copy(u, k, NEAR, 6, FAR, opp).start()
             to_partner(u, k, NEAR).start()
 
     def relay_across(u, role, ks=None):
         for k in ks or pieces_of(u):
             arrived(u, k, role)
-            if u >= 3:
-                @pl.when(is_mid)
-                def _():
-                    w_copy(u, k, role, 5 + role, role, near).start()
+
+            @pl.when(is_mid)
+            def _():
+                w_copy(u, k, role, 5 + role, role, near).start()
             to_partner(u, k, role).start()
 
     def relay_opp(u, ks=None):
@@ -214,14 +218,38 @@
         return tok.at[:, pl.ds(pl.multiple_of(j * feats, feats), feats)]
 
     def tok_local(j):
-        return pltpu.make_async_copy(tok_cols(j), xr.at[1, j], sem_tok.at[j])
-
-    def tok_part(h):
-        cols = pl.ds(pl.multiple_of(t * feats, feats), feats)
-        return remote(
-            tok.at[pl.ds(h * half, half), cols], xr.at[0, t, pl.ds(h * half, half)],
-            tok_send.at[h], tok_recv.at[h], near, t,
-        )
+        return pltpu.make_async_copy(tok_cols(j), xr.at[j], sem_tok.at[j])
+
+    def tok_quarter(of_half):
+        start = of_half * (width // 2) + t * quarter
+        return tok.at[:, pl.ds(pl.multiple_of(start, quarter), quarter)]
+
+    def end_tok():
+        return remote(tok_quarter(own_half), xq.at[0, t], t_send.at[0], t_recv.at[0], near, t)
+
+    def mid_tok():
+        return remote(tok_quarter(1 - own_half), xq.at[2, t], t_send.at[0], t_recv.at[2], opp, t)
+
+    def to_stage(h):
+        span = pl.ds(h * half, half)
+        a = tok_quarter(1 - own_half).at[span]
+        return remote(a, stage.at[span], t_send.at[1], t_recv.at[3 + h], near, t)
+
+    def from_stage(h):
+        span = pl.ds(h * half, half)
+        return remote(stage.at[span], xq.at[1, t, span], t_send.at[1], t_recv.at[1], opp, t)
+
+    def tok_arrived(i):
+        remote(stage, stage, t_send.at[0], t_recv.at[i], partner, t).wait_recv()
+
+    def part_sum(m, b):
+        return remote(cbuf.at[m, b], cin.at[m, b], c_send.at[m], c_recv.at[m], opp, t)
+
+    def part_sums(m):
+        return remote(cbuf.at[m], cin.at[m], c_send.at[m], c_recv.at[m], opp, t)
+
+    def squares_copy():
+        return remote(ss.at[1], ss.at[0], s_send, s_recv, near, t)
 
     def end_part(h):
         return remote(
@@ -274,48 +302,83 @@
         def drain(self):
             self.whole(3, 0).wait_send()
 
-    gather_tok = Gather(0, xr.at[0])
+    gather_tok = (Gather(0, xq.at[0]), Gather(4, xq.at[1]), Gather(5, xq.at[2]))
     gather_gat = (Gather(1, gat.at[0]), Gather(3, gat.at[1]))
     gather_x = Gather(2, x1)
 
-    def scale(layer, source, b, j):
+    def row_tiles(body):
         step = 64
 
         def tile(r, carry):
-            span = pl.ds(pl.multiple_of(r * step, step), step)
-            x = source[j, span, :].astype(f32)
-            sq = x * x
-            part = sq[:, :128]
-            for q in range(1, feats // 128):
-                part = part + sq[:, 128 * q : 128 * (q + 1)]
-            ss[b, span, :] += part
+            body(pl.ds(pl.multiple_of(r * step, step), step))
+            return carry
+
+        lax.fori_loop(0, rows // step, tile, 0)
+
+    def lane_sums(x):
+        sq = x * x
+        part = sq[:, :128]
+        for q in range(1, x.shape[1] // 128):
+            part = part + sq[:, 128 * q : 128 * (q + 1)]
+        return part
+
+    def squares(b):
+        ss[b] = jnp.zeros(ss.shape[1:], f32)
+
+        def one(j, carry):
+            def body(span):
+                ss[b, span, :] += lane_sums(xr[j, span, :].astype(f32))
+            row_tiles(body)
+            return carry
+
+        lax.fori_loop(0, n_tp, one, 0)
+
+    def scale(j):
+        def body(span):
+            x = x1[j, span, :].astype(f32)
+            ss[0, span, :] += lane_sums(x)
             cols = pl.ds(pl.multiple_of(j * feats, feats), feats)
-            scl[b, j, span, :] = (x * gain[layer : layer + 1, cols]).astype(bf16)
-            return carry
-
-        lax.fori_loop(0, rows // step, tile, 0)
-
-    def project(layer, m, sources, first):
-        blocks = (0, 1) if layer == 0 else (0,)
+            scl[j, span, :] = (x * gain[1:2, cols]).astype(bf16)
+        row_tiles(body)
+
+    def scale_part(load, block, j):
+        at = pl.multiple_of(j * quarter, quarter)
+        cols = pl.ds(pl.multiple_of(own_half * (width // 2) + at, quarter), quarter)
+
+        def body(span):
+            sclh[block, span, pl.ds(at, quarter)] = (load(span).astype(f32) * gain[0:1, cols]).astype(bf16)
+        row_tiles(body)
+
+    def scale_sent(i, j):
+        scale_part(lambda span: xq[i, j, span, :], (0, 2, 3)[i], j)
+
+    def half_dot(m, block):
         depth = win.shape[2]
-
-        def tile(b, carry):
-            total = None
-            for role in sources:
-                z = lax.div(source_of[role], 2)
-                w = win[3 * layer + m, pl.ds(2 * z, 2)].reshape(2 * depth, win.shape[3])
-                dot = jnp.dot(scl[b, z], w, preferred_element_type=f32)
-                total = dot if total is None else total + dot
-            if first:
-                acc[m, b] = total
-            else:
-                acc[m, b] += total
-            return carry
-
-        if len(blocks) == 1:
-            tile(0, 0)
+        sources = pl.ds(own_half * (n_sp // 2), n_sp // 2)
+        w = win[m, sources].reshape(n_sp // 2 * depth, win.shape[3])
+        return jnp.dot(sclh[block], w, preferred_element_type=f32)
+
+    def send_part_sum(m, b):
+        cbuf[m, b] = half_dot(m, 2 + b).astype(bf16)
+        part_sum(m, b).start()
+
+    def add_part_sums(m):
+        part_sums(m).wait_recv()
+        for b in range(2):
+            acc[m, b] += cin[m, b].astype(f32)
+
+    def project(m, sources, first):
+        depth = win.shape[2]
+        total = None
+        for role in sources:
+            z = lax.div(source_of[role], 2)
+            w = win[3 + m, pl.ds(2 * z, 2)].reshape(2 * depth, win.shape[3])
+            dot = jnp.dot(scl[z], w, preferred_element_type=f32)
+            total = dot if total is None else total + dot
+        if first:
+            acc[m, 0] = total
         else:
-            lax.fori_loop(0, len(blocks), tile, 0)
+            acc[m, 0] += total
 
     def inv_of(b):
         return lax.rsqrt(jnp.sum(ss[b], axis=-1, keepdims=True) / width + eps)
@@ -364,54 +427,89 @@
 
     @pl.when(is_mid)
     def _():
-        for u in FIRST[:3]:
-            send_opp(u)
-        for u in FIRST + SECOND:
+        mid_tok().start()
+        for u in FIRST + SHARED:
             send_partner(u)
-        for u in FIRST[3:] + SECOND:
+        for u in SHARED:
             send_near(u)
         for j in range(n_tp):
             tok_local(j).start()
-        for u in FIRST + SECOND:
+        for u in FIRST + SHARED:
             local_w(u).start()
-        ss[...] = jnp.zeros(ss.shape, f32)
         for j in range(n_tp):
             tok_local(j).wait()
+        squares(1)
 
         def scale_own(j, carry):
-            scale(0, xr.at[1], 1, j)
+            piece_of = own_half * (n_tp // 2) + lax.div(j, 2)
+            cols = pl.ds(pl.multiple_of(lax.rem(j, 2) * quarter, quarter), quarter)
+            scale_part(lambda span: xr[piece_of, span, cols], 1, j)
             return carry
 
         lax.fori_loop(0, n_tp, scale_own, 0)
+        own_end, far_end, far_mid = gather_tok
+        for h in range(2):
+            to_stage(h).wait_recv()
+            from_stage(h).start()
+        send_opp(BACK)
+        send_opp(SECOND[0])
+        tok_arrived(2)
+        far_mid.start_all()
+        scale_sent(2, t)
+        far_mid.forward(0)
+        far_mid.forward(1)
+        tok_arrived(1)
+        far_end.start_all()
+        far_mid.beside()
+        scale_sent(2, tx)
+        scale_sent(2, ty)
+        far_mid.across()
+        scale_sent(2, td)
         relay_near(INNER)
-        send_opp(BACK)
-        relay_opp(INNER)
-        for h in range(2):
-            tok_part(h).wait_recv()
-            gather_tok.start(h)
-            relay_opp((VALUE, OUTER)[h])
-        gather_tok.forward(0)
+        scale_sent(1, t)
+        relay_opp(BACK)
+
+        def have(u):
+            local_w(u).wait()
+            settle(u, OWN)
+            settle(u, NEAR)
+
+        have(INNER)
+        send_part_sum(INNER, 1)
+        far_end.forward(0)
+        far_end.forward(1)
+        tok_arrived(0)
+        own_end.start_all()
+        scale_sent(0, t)
+        far_end.beside()
+        scale_sent(1, tx)
+        scale_sent(1, ty)
         relay_near(VALUE)
-        relay_far(INNER)
-        scale(0, xr.at[0], 0, t)
-        gather_tok.forward(1)
+        relay_opp(SECOND[0])
+        have(VALUE)
+        send_part_sum(VALUE, 1)
+        far_end.across()
+        scale_sent(1, td)
+        send_part_sum(INNER, 0)
+        send_part_sum(VALUE, 0)
+        own_end.forward(0)
+        own_end.forward(1)
         relay_near(OUTER)
-        relay_opp(BACK)
-        gather_tok.beside()
-        scale(0, xr.at[0], 0, tx)
-        scale(0, xr.at[0], 0, ty)
-        gather_tok.across()
-        scale(0, xr.at[0], 0, td)
-        for u in FIRST[:3]:
-            local_w(u).wait()
-            for role in (OWN, NEAR, OPP):
-                settle(u, role)
-        settle(INNER, FAR)
-        project(0, INNER, (OWN, NEAR, OPP, FAR), True)
-        project(0, VALUE, (OWN, NEAR, OPP), True)
-        relay_far(VALUE)
-        settle(VALUE, FAR)
-        project(0, VALUE, (FAR,), False)
+        have(OUTER)
+        send_part_sum(OUTER, 1)
+        send_part_sum(OUTER, 0)
+        own_end.beside()
+        scale_sent(0, tx)
+        scale_sent(0, ty)
+        own_end.across()
+        scale_sent(0, td)
+        for m in FIRST:
+            for b in range(2):
+                acc[m, b] = half_dot(m, b)
+        relay_near(BACK)
+        add_part_sums(INNER)
+        add_part_sums(VALUE)
+        squares_copy().wait_recv()
         for b in range(2):
             mix(b, b)
 
@@ -428,11 +526,9 @@
         @pl.when(jnp.logical_and(core == 1, jnp.logical_not(left)))
         def _():
             tail_copy(1, 0, 0, partner).start()
-        relay_near(BACK)
-        for u in SECOND[:3]:
-            send_opp(u)
-        project(0, OUTER, (OWN, NEAR, OPP), True)
-        relay_far(OUTER)
+        send_opp(SECOND[1])
+        send_opp(SECOND[2])
+        add_part_sums(OUTER)
         for b in range(2):
             if b == 0:
                 start_of_all = s == 2
@@ -447,39 +543,46 @@
             else:
                 tail_copy(1, 1, 1, partner).wait_recv()
             convolve(0, b, b)
-        settle(OUTER, FAR)
-        project(0, OUTER, (FAR,), False)
-        gat_end[...] = gate(0)
-        for h in range(2):
-            end_part(h).start()
+            if b == 0:
+                gat_end[...] = gate(0)
+                for h in range(2):
+                    end_part(h).start()
         gat[0, t] = gate(1)
         gather_gat[0].start_all()
-        relay_near(SECOND[0])
+        relay_far(BACK, (0,))
         gather_gat[0].forward(0)
         gather_gat[0].forward(1)
-        relay_far(BACK)
+        relay_near(SECOND[0])
+        relay_far(BACK, (1,))
 
     @pl.when(is_end)
     def _():
-        send_near(INNER)
         for h in range(2):
-            tok_part(h).start()
-        for u in FIRST[1:] + SECOND:
+            to_stage(h).start()
+        end_tok().start()
+        for u in FIRST + (BACK,):
             send_near(u)
-        for u in FIRST[3:] + SECOND:
+        for j in range(n_tp):
+            tok_local(j).start()
+        for u in SHARED:
             send_partner(u)
-        tok_local(t).start()
-        for u in FIRST[3:] + SECOND:
+        for u in SHARED:
             local_w(u).start()
-        tok_local(t).wait()
-        for u in FIRST[3:] + SECOND:
+        for j in range(n_tp):
+            tok_local(j).wait()
+        squares(1)
+        squares_copy().start()
+        for u in SECOND:
+            send_near(u)
+        for u in SHARED:
             relay_near(u)
         relay_opp(BACK)
+        relay_opp(SECOND[0])
         for h in range(2):
             end_part(h).wait_recv()
             gather_gat[0].start(h)
+        gather_gat[0].forward(0)
         relay_far(BACK, (0,))
-        gather_gat[0].forward(0)
         gather_gat[0].forward(1)
         relay_far(BACK, (1,))
 
@@ -490,43 +593,41 @@
         settle(BACK, role)
 
     def finish_first(cols):
-        total = xr[1, t, :, cols].astype(f32) + back_dot(0, (OWN, NEAR, OPP, FAR), cols)
+        total = xr[t, :, cols].astype(f32) + back_dot(0, (OWN, NEAR, OPP, FAR), cols)
         x1[t, :, cols] = total.astype(bf16)
 
     by_columns(finish_first)
     gather_x.start_all()
+    relay_opp(SECOND[1])
 
     @pl.when(is_mid)
     def _():
         relay_near(SECOND[1])
-    relay_opp(SECOND[0])
+    ss[0] = jnp.zeros(ss.shape[1:], f32)
+    scale(t)
+    relay_opp(SECOND[2])
 
     @pl.when(is_mid)
     def _():
         relay_near(SECOND[2])
-    ss[0] = jnp.zeros(ss.shape[1:], f32)
-    scale(1, x1, 0, t)
-    relay_opp(SECOND[1])
     gather_x.forward(0)
     gather_x.forward(1)
-    relay_opp(SECOND[2])
+    relay_far(SECOND[0])
     gather_x.beside()
-    scale(1, x1, 0, tx)
-    scale(1, x1, 0, ty)
-    relay_far(SECOND[0])
+    scale(tx)
+    scale(ty)
+    relay_far(SECOND[1])
     gather_x.across()
-    scale(1, x1, 0, td)
+    scale(td)
     for u in SECOND[:3]:
         local_w(u).wait()
         for role in (OWN, NEAR, OPP):
             settle(u, role)
-    for u in SECOND[:3]:
-        project(1, u % 4, (OWN, NEAR, OPP), True)
     settle(SECOND[0], FAR)
-    project(1, INNER, (FAR,), False)
-    relay_far(SECOND[1])
+    project(INNER, (OWN, NEAR, OPP, FAR), True)
+    project(VALUE, (OWN, NEAR, OPP), True)
     settle(SECOND[1], FAR)
-    project(1, VALUE, (FAR,), False)
+    project(VALUE, (FAR,), False)
     mix(0, 2)
 
     @pl.when(s < n_sp - 1)
@@ -538,6 +639,7 @@
     def _():
         send_opp(last)
         relay_near(last)
+    project(OUTER, (OWN, NEAR, OPP), True)
     relay_far(SECOND[2])
 
     @pl.when(is_mid)
@@ -553,7 +655,7 @@
         tail_copy(2, 2, 2, partner).wait_recv()
     convolve(1, 0, 2)
     settle(SECOND[2], FAR)
-    project(1, OUTER, (FAR,), False)
+    project(OUTER, (FAR,), False)
     gat[1, t] = gate(0)
     gather_gat[1].start_all()
 
@@ -595,11 +697,16 @@
 
     @pl.when(is_mid)
     def _():
-        for kind in (0, 1, 2, 3, 4, 6):
+        for kind in (0, 1):
             sent(kind, units)
-        for kind in (5, 7, 8):
+        for kind in (2, 3, 4, 5, 6, 7, 8):
             sent(kind, some)
-        gather_tok.drain()
+        for g in gather_tok:
+            g.drain()
+        for i in range(2):
+            remote(stage, stage, t_send.at[i], t_recv.at[0], partner, t).wait_send()
+        for m in range(3):
+            part_sums(m).wait_send()
         for h in range(2):
             end_part(h).wait_send()
 
@@ -622,8 +729,9 @@
         for kind in (0, 1, 2, 3):
             sent(kind, some)
         sent(5, units)
-        for h in range(2):
-            tok_part(h).wait_send()
+        for i in range(2):
+            remote(stage, stage, t_send.at[i], t_recv.at[0], partner, t).wait_send()
+        squares_copy().wait_send()
     gather_gat[0].drain()
     gather_x.drain()
     gather_gat[1].drain()
@@ -655,9 +763,14 @@
         scratch_shapes=[
             pltpu.VMEM((layers, width), f32),
             pltpu.VMEM(taps.shape[1:2] + taps.shape[:1] + taps.shape[2:], f32),
-            pltpu.VMEM((2, n_tp, rows, feats), bf16),
             pltpu.VMEM((n_tp, rows, feats), bf16),
-            pltpu.VMEM((2, n_tp, rows, feats), bf16),
+            pltpu.VMEM((3, n_tp, rows, width // 2 // n_tp), bf16),
+            pltpu.VMEM((rows, width // 2 // n_tp), bf16),
+            pltpu.VMEM((n_tp, rows, feats), bf16),
+            pltpu.VMEM((n_tp, rows, feats), bf16),
+            pltpu.VMEM((4, rows, width // 2), bf16),
+            pltpu.VMEM((3, 2, rows, chans), bf16),
+            pltpu.VMEM((3, 2, rows, chans), bf16),
             pltpu.VMEM((3 * layers, n_sp, depth, chans), bf16),
             pltpu.VMEM((layers, n_sp, back_rows, feats), bf16),
             pltpu.VMEM((3, 2, rows, chans), f32),
@@ -671,12 +784,16 @@
             dma((4 * layers,)),
             dma((n_tp,)),
             dma((2,)),
-            dma((2,)),
+            dma((5,)),
+            dma((3,)),
+            dma((3,)),
+            dma,
+            dma,
             dma((KINDS,)),
             dma((chunks, 3)),
             dma((4 * layers, 4)),
-            dma((4,)),
-            dma((4, 4)),
+            dma((6,)),
+            dma((6, 4)),
             dma((3,)),
             dma((3,)),
             dma((2,)),

time: 108 us -> 103 us (0.954)
  Pallas kernels: 107 us -> 101 us
    pallas_call x1, Pallas kernels: 107 us -> 101 us  [fused(): pl.pallas_call(mixer_kernel, out_shape=jax.ShapeDtypeStruct((rows, feats)...]
where the time goes in v5:
time: 103 us; the launch traced here: 102 us
  Pallas kernels  101 us (98%)
    pallas_call x1, Pallas kernels, fused(): pl.pallas_call(mixer_kernel, out_shape=jax.ShapeDtypeStruct((rows, feats)...  101 us

profile of v5, /device:TPU:1, one launch (start us, length us, event | category | flops | bytes accessed | tf_op | source)
XLA Modules:
  0.0 101.7 jit_solution(2833784889261152326)
XLA Ops:
  0.0 100.9 %mixer.1 = bf16[256,1024]{1,0:T(8,128)(2,1)S(1)} custom-call(bf16[256,4096]{1,0:T(8,128)(2,1)} %tok.1, f32[2,4096]{1,0:T(2,128)} %gain_hbm.1, bf16[2,512,256]{2,1,0:T(8,128)(2,1)} %w_outer.1, bf16[2,512,256]{2,1,0:T(8,128)(2,1)} %w_inner.1, bf16[2,512,256]{2,1,0:T(8,128)(2,1)} %w_value.1, bf16[2,128,1024]{2,1,0:T(8,128)(2,1)} %w_back.1, f32[3,2,256]{2,1,0:T(2,128)} %bitcast.1), custom_call_target="tpu_custom_call" | custom-call | tf_op jit(solution)/shard_map/mixer/pallas_call | solution.py:758
  100.9 0.8 copy.9

commit v6 on v5

--- a/solution.py
+++ b/solution.py
@@ -19,6 +19,7 @@
 SHARED = (BACK,) + SECOND
 PIECES = (1, 1, 1, 2, 4, 2, 2, 4)
 KINDS = 9
+GROUP = 8
 
 
 def shifted(block, axis, distance):
@@ -157,7 +158,7 @@
     def to_partner(u, k, role):
         to = piece(held_w(u, source_of[role]), u, k)
         a = piece(own_w(u), u, k) if role == OWN else to
-        return remote(a, to, w_send.at[role], p_recv.at[u, role], partner, t)
+        return remote(a, to, w_send.at[role], p_recv.at[group_of(u, role)], partner, t)
 
     def pieces_of(u):
         return range(PIECES[u])
@@ -203,22 +204,39 @@
     def relay_far(u, ks=None):
         relay_across(u, FAR, ks)
 
-    def settle(u, role):
-        to = held_w(u, source_of[role] + flip)
-        remote(to, to, w_send.at[0], p_recv.at[u, role], partner, t).wait_recv()
+    counts = {INNER: 2, VALUE: 2, OUTER: 2, BACK: 4, GROUP: 9, GROUP + 1: 1, GROUP + 2: 1, GROUP + 3: 1, 7: 3, GROUP + 4: 1}
+
+    def group_of(u, role):
+        if u <= BACK:
+            return u
+        if u == 7:
+            return GROUP + 4 if role == FAR else 7
+        return GROUP + 1 + SECOND.index(u) if role == FAR else GROUP
+
+    def settle(group):
+        count = counts[group]
+        ref = win.at[pl.ds(0, 3), pl.ds(0, 3)] if count == 9 else win.at[0, pl.ds(0, count)]
+        remote(ref, ref, w_send.at[0], p_recv.at[group], partner, t).wait_recv()
 
     def sent(kind, count):
         ref = win.at[0, pl.ds(0, count)]
-        remote(ref, ref, w_send.at[kind], p_recv.at[0, 0], partner, t).wait_send()
+        remote(ref, ref, w_send.at[kind], p_recv.at[0], partner, t).wait_send()
 
     def local_w(u):
-        return pltpu.make_async_copy(own_w(u), held_w(u, s), sem_local.at[u])
+        return pltpu.make_async_copy(own_w(u), held_w(u, s), sem_local)
+
+    def local_w_wait(count):
+        ref = win.at[0, pl.ds(0, count)]
+        pltpu.make_async_copy(ref, ref, sem_local).wait()
 
     def tok_cols(j):
         return tok.at[:, pl.ds(pl.multiple_of(j * feats, feats), feats)]
 
     def tok_local(j):
-        return pltpu.make_async_copy(tok_cols(j), xr.at[j], sem_tok.at[j])
+        return pltpu.make_async_copy(tok_cols(j), xr.at[j], sem_tok)
+
+    def tok_local_wait():
+        pltpu.make_async_copy(xr, xr, sem_tok).wait()
 
     def tok_quarter(of_half):
         start = of_half * (width // 2) + t * quarter
@@ -418,12 +436,8 @@
 
     def by_columns(body):
         step = 256
-
-        def tile(c, carry):
-            body(pl.ds(pl.multiple_of(c * step, step), step))
-            return carry
-
-        lax.fori_loop(0, feats // step, tile, 0)
+        for c in range(feats // step):
+            body(pl.ds(c * step, step))
 
     @pl.when(is_mid)
     def _():
@@ -436,8 +450,7 @@
             tok_local(j).start()
         for u in FIRST + SHARED:
             local_w(u).start()
-        for j in range(n_tp):
-            tok_local(j).wait()
+        tok_local_wait()
         squares(1)
 
         def scale_own(j, carry):
@@ -447,6 +460,7 @@
             return carry
 
         lax.fori_loop(0, n_tp, scale_own, 0)
+        local_w_wait(units)
         own_end, far_end, far_mid = gather_tok
         for h in range(2):
             to_stage(h).wait_recv()
@@ -469,12 +483,7 @@
         scale_sent(1, t)
         relay_opp(BACK)
 
-        def have(u):
-            local_w(u).wait()
-            settle(u, OWN)
-            settle(u, NEAR)
-
-        have(INNER)
+        settle(INNER)
         send_part_sum(INNER, 1)
         far_end.forward(0)
         far_end.forward(1)
@@ -486,7 +495,7 @@
         scale_sent(1, ty)
         relay_near(VALUE)
         relay_opp(SECOND[0])
-        have(VALUE)
+        settle(VALUE)
         send_part_sum(VALUE, 1)
         far_end.across()
         scale_sent(1, td)
@@ -495,7 +504,7 @@
         own_end.forward(0)
         own_end.forward(1)
         relay_near(OUTER)
-        have(OUTER)
+        settle(OUTER)
         send_part_sum(OUTER, 1)
         send_part_sum(OUTER, 0)
         own_end.beside()
@@ -506,7 +515,6 @@
         for m in FIRST:
             for b in range(2):
                 acc[m, b] = half_dot(m, b)
-        relay_near(BACK)
         add_part_sums(INNER)
         add_part_sums(VALUE)
         squares_copy().wait_recv()
@@ -526,6 +534,7 @@
         @pl.when(jnp.logical_and(core == 1, jnp.logical_not(left)))
         def _():
             tail_copy(1, 0, 0, partner).start()
+        relay_near(BACK)
         send_opp(SECOND[1])
         send_opp(SECOND[2])
         add_part_sums(OUTER)
@@ -568,12 +577,12 @@
             send_partner(u)
         for u in SHARED:
             local_w(u).start()
-        for j in range(n_tp):
-            tok_local(j).wait()
+        tok_local_wait()
         squares(1)
         squares_copy().start()
         for u in SECOND:
             send_near(u)
+        local_w_wait(units - 3)
         for u in SHARED:
             relay_near(u)
         relay_opp(BACK)
@@ -588,9 +597,11 @@
 
     gather_gat[0].beside()
     gather_gat[0].across()
-    local_w(BACK).wait()
-    for role in (OWN, NEAR, OPP, FAR):
-        settle(BACK, role)
+    settle(BACK)
+
+    @pl.when(is_mid)
+    def _():
+        relay_opp(SECOND[1], (0,))
 
     def finish_first(cols):
         total = xr[t, :, cols].astype(f32) + back_dot(0, (OWN, NEAR, OPP, FAR), cols)
@@ -598,7 +609,11 @@
 
     by_columns(finish_first)
     gather_x.start_all()
-    relay_opp(SECOND[1])
+
+    @pl.when(is_end)
+    def _():
+        relay_opp(SECOND[1], (0,))
+    relay_opp(SECOND[1], (1,))
 
     @pl.when(is_mid)
     def _():
@@ -619,15 +634,20 @@
     relay_far(SECOND[1])
     gather_x.across()
     scale(td)
-    for u in SECOND[:3]:
-        local_w(u).wait()
-        for role in (OWN, NEAR, OPP):
-            settle(u, role)
-    settle(SECOND[0], FAR)
+    settle(GROUP)
+    def early_far(k):
+        @pl.when(is_mid)
+        def _():
+            relay_far(SECOND[2], (k,))
+
+    early_far(0)
+    settle(GROUP + 1)
     project(INNER, (OWN, NEAR, OPP, FAR), True)
+    early_far(1)
     project(VALUE, (OWN, NEAR, OPP), True)
-    settle(SECOND[1], FAR)
+    settle(GROUP + 2)
     project(VALUE, (FAR,), False)
+    early_far(2)
     mix(0, 2)
 
     @pl.when(s < n_sp - 1)
@@ -640,7 +660,11 @@
         send_opp(last)
         relay_near(last)
     project(OUTER, (OWN, NEAR, OPP), True)
-    relay_far(SECOND[2])
+
+    @pl.when(is_end)
+    def _():
+        relay_far(SECOND[2], (0, 1, 2))
+    relay_far(SECOND[2], (3,))
 
     @pl.when(is_mid)
     def _():
@@ -654,14 +678,14 @@
     def _():
         tail_copy(2, 2, 2, partner).wait_recv()
     convolve(1, 0, 2)
-    settle(SECOND[2], FAR)
+    settle(GROUP + 3)
     project(OUTER, (FAR,), False)
     gat[1, t] = gate(0)
     gather_gat[1].start_all()
 
     @pl.when(is_end)
     def _():
-        relay_opp(last)
+        relay_opp(last, (0, 1))
 
     @pl.when(is_mid)
     def _():
@@ -669,14 +693,16 @@
     gather_gat[1].forward(0)
     gather_gat[1].forward(1)
 
+    @pl.when(is_end)
+    def _():
+        relay_opp(last, (2, 3))
+
     @pl.when(is_mid)
     def _():
         relay_far(last, (2, 3))
     gather_gat[1].beside()
     gather_gat[1].across()
-    local_w(last).wait()
-    for role in (OWN, NEAR, OPP):
-        settle(last, role)
+    settle(last)
 
     def start_last(cols):
         bacc[:, cols] = x1[t, :, cols].astype(f32) + back_dot(1, (OWN, NEAR, OPP), cols)
@@ -686,7 +712,7 @@
     @pl.when(is_end)
     def _():
         relay_far(last)
-    settle(last, FAR)
+    settle(GROUP + 4)
 
     def finish_last(cols):
         out[:, cols] = (bacc[:, cols] + back_dot(1, (FAR,), cols)).astype(bf16)
@@ -781,8 +807,8 @@
             pltpu.VMEM((3, rows, chans), bf16),
             pltpu.VMEM((3, 16, chans), bf16),
             dma((2,)),
-            dma((4 * layers,)),
-            dma((n_tp,)),
+            dma,
+            dma,
             dma((2,)),
             dma((5,)),
             dma((3,)),
@@ -791,7 +817,7 @@
             dma,
             dma((KINDS,)),
             dma((chunks, 3)),
-            dma((4 * layers, 4)),
+            dma((GROUP + 5,)),
             dma((6,)),
             dma((6, 4)),
             dma((3,)),

time: 103 us -> 100 us (0.971); the launches traced: 102 us -> 100 us
  Pallas kernels: 101 us -> 99.5 us
    pallas_call x1, Pallas kernels: 101 us -> 99.5 us  [fused(): pl.pallas_call(mixer_kernel, out_shape=jax.ShapeDtypeStruct((rows, feats)...]
where the time goes in v6:
time: 100 us
  Pallas kernels  99.5 us (100%)
    pallas_call x1, Pallas kernels, fused(): pl.pallas_call(mixer_kernel, out_shape=jax.ShapeDtypeStruct((rows, feats)...  99.5 us

profile of v6, /device:TPU:1, one launch (start us, length us, event | category | flops | bytes accessed | tf_op | source)
XLA Modules:
  0.0 100.3 jit_solution(9578128016402538783)
XLA Ops:
  0.0 99.5 %mixer.1 = bf16[256,1024]{1,0:T(8,128)(2,1)S(1)} custom-call(bf16[256,4096]{1,0:T(8,128)(2,1)} %tok.1, f32[2,4096]{1,0:T(2,128)} %gain_hbm.1, bf16[2,512,256]{2,1,0:T(8,128)(2,1)} %w_outer.1, bf16[2,512,256]{2,1,0:T(8,128)(2,1)} %w_inner.1, bf16[2,512,256]{2,1,0:T(8,128)(2,1)} %w_value.1, bf16[2,128,1024]{2,1,0:T(8,128)(2,1)} %w_back.1, f32[3,2,256]{2,1,0:T(2,128)} %bitcast.1), custom_call_target="tpu_custom_call" | custom-call | tf_op jit(solution)/shard_map/mixer/pallas_call | solution.py:784
  99.5 0.8 copy.9

commit v7 on v6

--- a/solution.py
+++ b/solution.py
@@ -18,7 +18,6 @@
 SECOND = tuple(4 + m for m in FIRST + (BACK,))
 SHARED = (BACK,) + SECOND
 PIECES = (1, 1, 1, 2, 4, 2, 2, 4)
-KINDS = 9
 GROUP = 8
 
 
@@ -69,8 +68,10 @@
     return resid
 
 
-def first_chunk(u):
-    return sum(PIECES[:u])
+def chunk(u, k, role):
+    if u < BACK:
+        return u
+    return 3 + 3 * (sum(PIECES[BACK:u]) + k) + role - 1
 
 
 def mixer_kernel(
@@ -153,22 +154,22 @@
     def w_copy(u, k, role, kind, to_role, target):
         to = piece(held_w(u, source_of[role]), u, k)
         a = piece(own_w(u), u, k) if role == OWN else to
-        return remote(a, to, w_send.at[kind], w_recv.at[first_chunk(u) + k, to_role - 1], target, t)
+        return remote(a, to, w_send.at[min(kind // 2, 1)], w_recv.at[chunk(u, k, to_role)], target, t)
 
     def to_partner(u, k, role):
         to = piece(held_w(u, source_of[role]), u, k)
         a = piece(own_w(u), u, k) if role == OWN else to
-        return remote(a, to, w_send.at[role], p_recv.at[group_of(u, role)], partner, t)
+        return remote(a, to, w_send.at[role // 2], p_recv.at[group_of(u, role)], partner, t)
 
     def pieces_of(u):
         return range(PIECES[u])
 
     def arrived(u, k, role):
         to = piece(held_w(u, source_of[role]), u, k)
-        remote(to, to, w_send.at[0], w_recv.at[first_chunk(u) + k, role - 1], partner, t).wait_recv()
-
-    def send_opp(u):
-        for k in pieces_of(u):
+        remote(to, to, w_send.at[0], w_recv.at[chunk(u, k, role)], partner, t).wait_recv()
+
+    def send_opp(u, ks=None):
+        for k in ks or pieces_of(u):
             w_copy(u, k, OWN, 4, OPP, opp).start()
 
     def send_near(u):
@@ -218,9 +219,9 @@
         ref = win.at[pl.ds(0, 3), pl.ds(0, 3)] if count == 9 else win.at[0, pl.ds(0, count)]
         remote(ref, ref, w_send.at[0], p_recv.at[group], partner, t).wait_recv()
 
-    def sent(kind, count):
-        ref = win.at[0, pl.ds(0, count)]
-        remote(ref, ref, w_send.at[kind], p_recv.at[0], partner, t).wait_send()
+    def sent(slot, planes_of, count):
+        ref = win.at[pl.ds(0, planes_of), pl.ds(0, count)]
+        remote(ref, ref, w_send.at[slot], p_recv.at[0], partner, t).wait_send()
 
     def local_w(u):
         return pltpu.make_async_copy(own_w(u), held_w(u, s), sem_local)
@@ -261,10 +262,10 @@
         remote(stage, stage, t_send.at[0], t_recv.at[i], partner, t).wait_recv()
 
     def part_sum(m, b):
-        return remote(cbuf.at[m, b], cin.at[m, b], c_send.at[m], c_recv.at[m], opp, t)
+        return remote(cbuf.at[m, b], cin.at[m, b], c_send, c_recv.at[m], opp, t)
 
     def part_sums(m):
-        return remote(cbuf.at[m], cin.at[m], c_send.at[m], c_recv.at[m], opp, t)
+        return remote(cbuf.at[m], cin.at[m], c_send, c_recv.at[m], opp, t)
 
     def squares_copy():
         return remote(ss.at[1], ss.at[0], s_send, s_recv, near, t)
@@ -272,17 +273,17 @@
     def end_part(h):
         return remote(
             gat_end.at[pl.ds(h * half, half)], gat.at[0, t, pl.ds(h * half, half)],
-            e_send.at[h], e_recv.at[h], near, t,
+            e_send, e_recv.at[h], near, t,
         )
 
     class Gather:
-        def __init__(self, g, buf):
-            self.g, self.buf = g, buf
+        def __init__(self, g, buf, joint=False):
+            self.g, self.buf, self.joint = g, buf, joint
 
         def part(self, block, h, k, target):
             size = self.buf.shape[1] // 2
             ref = self.buf.at[block, pl.ds(h * size, size)]
-            slot = (0, 1, 2, 2, 3, 3)[k]
+            slot = (0, 1, 2, 2, 2, 2)[k] if self.joint else (0, 1, 2, 2, 3, 3)[k]
             return remote(ref, ref, g_send.at[self.g], g_recv.at[self.g, slot], s, target)
 
         def whole(self, blocks, slot):
@@ -317,11 +318,14 @@
         def across(self):
             self.whole(1, 3).wait_recv()
 
+        def rest(self):
+            self.whole(2, 2).wait_recv()
+
         def drain(self):
             self.whole(3, 0).wait_send()
 
     gather_tok = (Gather(0, xq.at[0]), Gather(4, xq.at[1]), Gather(5, xq.at[2]))
-    gather_gat = (Gather(1, gat.at[0]), Gather(3, gat.at[1]))
+    gather_gat = (Gather(1, gat.at[0], True), Gather(3, gat.at[1], True))
     gather_x = Gather(2, x1)
 
     def row_tiles(body):
@@ -480,33 +484,32 @@
         far_mid.across()
         scale_sent(2, td)
         relay_near(INNER)
-        scale_sent(1, t)
-        relay_opp(BACK)
-
         settle(INNER)
         send_part_sum(INNER, 1)
         far_end.forward(0)
         far_end.forward(1)
+        relay_near(VALUE)
+        settle(VALUE)
+        send_part_sum(VALUE, 1)
+        relay_opp(BACK)
+        scale_sent(1, t)
+        far_end.beside()
+        scale_sent(1, tx)
+        scale_sent(1, ty)
+        relay_opp(SECOND[0])
         tok_arrived(0)
         own_end.start_all()
         scale_sent(0, t)
-        far_end.beside()
-        scale_sent(1, tx)
-        scale_sent(1, ty)
-        relay_near(VALUE)
-        relay_opp(SECOND[0])
-        settle(VALUE)
-        send_part_sum(VALUE, 1)
         far_end.across()
         scale_sent(1, td)
         send_part_sum(INNER, 0)
         send_part_sum(VALUE, 0)
+        relay_near(OUTER)
+        settle(OUTER)
         own_end.forward(0)
         own_end.forward(1)
-        relay_near(OUTER)
-        settle(OUTER)
+        send_part_sum(OUTER, 0)
         send_part_sum(OUTER, 1)
-        send_part_sum(OUTER, 0)
         own_end.beside()
         scale_sent(0, tx)
         scale_sent(0, ty)
@@ -537,25 +540,20 @@
         relay_near(BACK)
         send_opp(SECOND[1])
         send_opp(SECOND[2])
+        @pl.when(s == 2)
+        def _():
+            halo[0] = jnp.zeros(halo.shape[1:], bf16)
+
+        @pl.when(s != 2)
+        def _():
+            tail_copy(0, 0, 0, partner).wait_recv()
+        convolve(0, 0, 0)
         add_part_sums(OUTER)
-        for b in range(2):
-            if b == 0:
-                start_of_all = s == 2
-
-                @pl.when(start_of_all)
-                def _():
-                    halo[0] = jnp.zeros(halo.shape[1:], bf16)
-
-                @pl.when(jnp.logical_not(start_of_all))
-                def _():
-                    tail_copy(0, 0, 0, partner).wait_recv()
-            else:
-                tail_copy(1, 1, 1, partner).wait_recv()
-            convolve(0, b, b)
-            if b == 0:
-                gat_end[...] = gate(0)
-                for h in range(2):
-                    end_part(h).start()
+        gat_end[...] = gate(0)
+        for h in range(2):
+            end_part(h).start()
+        tail_copy(1, 1, 1, partner).wait_recv()
+        convolve(0, 1, 1)
         gat[0, t] = gate(1)
         gather_gat[0].start_all()
         relay_far(BACK, (0,))
@@ -568,9 +566,10 @@
     def _():
         for h in range(2):
             to_stage(h).start()
+        send_near(INNER)
+        send_near(VALUE)
         end_tok().start()
-        for u in FIRST + (BACK,):
-            send_near(u)
+        send_near(OUTER)
         for j in range(n_tp):
             tok_local(j).start()
         for u in SHARED:
@@ -580,7 +579,7 @@
         tok_local_wait()
         squares(1)
         squares_copy().start()
-        for u in SECOND:
+        for u in SHARED:
             send_near(u)
         local_w_wait(units - 3)
         for u in SHARED:
@@ -595,8 +594,7 @@
         gather_gat[0].forward(1)
         relay_far(BACK, (1,))
 
-    gather_gat[0].beside()
-    gather_gat[0].across()
+    gather_gat[0].rest()
     settle(BACK)
 
     @pl.when(is_mid)
@@ -640,6 +638,11 @@
         def _():
             relay_far(SECOND[2], (k,))
 
+    last = SECOND[3]
+
+    @pl.when(is_mid)
+    def _():
+        send_opp(last, (0, 1))
     early_far(0)
     settle(GROUP + 1)
     project(INNER, (OWN, NEAR, OPP, FAR), True)
@@ -653,11 +656,10 @@
     @pl.when(s < n_sp - 1)
     def _():
         tail_copy(2, 2, 2, s + 1).start()
-    last = SECOND[3]
-
-    @pl.when(is_mid)
-    def _():
-        send_opp(last)
+
+    @pl.when(is_mid)
+    def _():
+        send_opp(last, (2, 3))
         relay_near(last)
     project(OUTER, (OWN, NEAR, OPP), True)
 
@@ -700,8 +702,7 @@
     @pl.when(is_mid)
     def _():
         relay_far(last, (2, 3))
-    gather_gat[1].beside()
-    gather_gat[1].across()
+    gather_gat[1].rest()
     settle(last)
 
     def start_last(cols):
@@ -723,18 +724,14 @@
 
     @pl.when(is_mid)
     def _():
-        for kind in (0, 1):
-            sent(kind, units)
-        for kind in (2, 3, 4, 5, 6, 7, 8):
-            sent(kind, some)
+        sent(0, 2, units)
+        sent(1, some, 7)
         for g in gather_tok:
             g.drain()
         for i in range(2):
             remote(stage, stage, t_send.at[i], t_recv.at[0], partner, t).wait_send()
-        for m in range(3):
-            part_sums(m).wait_send()
-        for h in range(2):
-            end_part(h).wait_send()
+        remote(cbuf, cin, c_send, c_recv.at[0], partner, t).wait_send()
+        remote(gat_end, gat_end, e_send, e_recv.at[0], partner, t).wait_send()
 
         @pl.when(core == 0)
         def _():
@@ -752,9 +749,8 @@
 
     @pl.when(is_end)
     def _():
-        for kind in (0, 1, 2, 3):
-            sent(kind, some)
-        sent(5, units)
+        sent(0, 2, some)
+        sent(1, 3, 6)
         for i in range(2):
             remote(stage, stage, t_send.at[i], t_recv.at[0], partner, t).wait_send()
         squares_copy().wait_send()
@@ -774,7 +770,7 @@
     back_rows, feats = w_back.shape[1:]
     if 4 * layers != len(PIECES):
         return per_device(tokens, norm_gain, w_outer, w_inner, w_value, w_back, taps)
-    chunks = sum(PIECES)
+    chunks = 3 + 3 * sum(PIECES[BACK:])
     dma = pltpu.SemaphoreType.DMA
     hbm, vmem = pl.BlockSpec(memory_space=pl.ANY), pl.BlockSpec(memory_space=pltpu.VMEM)
     held = [
@@ -811,18 +807,18 @@
             dma,
             dma((2,)),
             dma((5,)),
-            dma((3,)),
+            dma,
             dma((3,)),
             dma,
             dma,
-            dma((KINDS,)),
-            dma((chunks, 3)),
+            dma((2,)),
+            dma((chunks,)),
             dma((GROUP + 5,)),
             dma((6,)),
             dma((6, 4)),
             dma((3,)),
             dma((3,)),
-            dma((2,)),
+            dma,
             dma((2,)),
         ],
         compiler_params=pltpu.CompilerParams(

time: 100 us -> 98.8 us (0.988)
  Pallas kernels: 99.5 us -> 97.6 us
    pallas_call x1, Pallas kernels: 99.5 us -> 97.6 us  [fused(): pl.pallas_call(mixer_kernel, out_shape=jax.ShapeDtypeStruct((rows, feats)...]
where the time goes in v7:
time: 98.8 us; the launch traced here: 98.4 us
  Pallas kernels  97.6 us (99%)
    pallas_call x1, Pallas kernels, fused(): pl.pallas_call(mixer_kernel, out_shape=jax.ShapeDtypeStruct((rows, feats)...  97.6 us

profile of v7, /device:TPU:1, one launch (start us, length us, event | category | flops | bytes accessed | tf_op | source)
XLA Modules:
  0.0 98.4 jit_solution(15301217459350290117)
XLA Ops:
  0.0 97.6 %mixer.1 = bf16[256,1024]{1,0:T(8,128)(2,1)S(1)} custom-call(bf16[256,4096]{1,0:T(8,128)(2,1)} %tok.1, f32[2,4096]{1,0:T(2,128)} %gain_hbm.1, bf16[2,512,256]{2,1,0:T(8,128)(2,1)} %w_outer.1, bf16[2,512,256]{2,1,0:T(8,128)(2,1)} %w_inner.1, bf16[2,512,256]{2,1,0:T(8,128)(2,1)} %w_value.1, bf16[2,128,1024]{2,1,0:T(8,128)(2,1)} %w_back.1, f32[3,2,256]{2,1,0:T(2,128)} %bitcast.1), custom_call_target="tpu_custom_call" | custom-call | tf_op jit(solution)/shard_map/mixer/pallas_call | solution.py:780
  97.6 0.8 copy.9

commit v8 on v7

--- a/solution.py
+++ b/solution.py
@@ -108,6 +108,21 @@
         pltpu.make_async_copy(gain_hbm, gain, sem_small.at[0]),
         pltpu.make_async_copy(taps_hbm, taps, sem_small.at[1]),
     )
+
+    ahead = (1 - own_half) * (n_tp // 2) + lax.div(t, 2)
+    ahead_cols = pl.ds(pl.multiple_of(lax.rem(t, 2) * quarter, quarter), quarter)
+
+    def tok_local(i):
+        j = lax.rem(ahead + i, n_tp)
+        cols = pl.ds(pl.multiple_of(j * feats, feats), feats)
+        return pltpu.make_async_copy(tok.at[:, cols], xr.at[j], sem_tok.at[min(i, 1)])
+
+    def tok_local_wait(slot, count):
+        ref = xr.at[pl.ds(0, count)]
+        pltpu.make_async_copy(ref, ref, sem_tok.at[slot]).wait()
+
+    for i in range(n_tp):
+        tok_local(i).start()
     for copy in small:
         copy.start()
     barrier = pltpu.get_barrier_semaphore()
@@ -230,15 +245,6 @@
         ref = win.at[0, pl.ds(0, count)]
         pltpu.make_async_copy(ref, ref, sem_local).wait()
 
-    def tok_cols(j):
-        return tok.at[:, pl.ds(pl.multiple_of(j * feats, feats), feats)]
-
-    def tok_local(j):
-        return pltpu.make_async_copy(tok_cols(j), xr.at[j], sem_tok)
-
-    def tok_local_wait():
-        pltpu.make_async_copy(xr, xr, sem_tok).wait()
-
     def tok_quarter(of_half):
         start = of_half * (width // 2) + t * quarter
         return tok.at[:, pl.ds(pl.multiple_of(start, quarter), quarter)]
@@ -247,11 +253,11 @@
         return remote(tok_quarter(own_half), xq.at[0, t], t_send.at[0], t_recv.at[0], near, t)
 
     def mid_tok():
-        return remote(tok_quarter(1 - own_half), xq.at[2, t], t_send.at[0], t_recv.at[2], opp, t)
+        return remote(xr.at[ahead, :, ahead_cols], xq.at[2, t], t_send.at[0], t_recv.at[2], opp, t)
 
     def to_stage(h):
         span = pl.ds(h * half, half)
-        a = tok_quarter(1 - own_half).at[span]
+        a = xr.at[ahead, span, ahead_cols]
         return remote(a, stage.at[span], t_send.at[1], t_recv.at[3 + h], near, t)
 
     def from_stage(h):
@@ -445,16 +451,15 @@
 
     @pl.when(is_mid)
     def _():
+        tok_local_wait(0, 1)
         mid_tok().start()
         for u in FIRST + SHARED:
             send_partner(u)
         for u in SHARED:
             send_near(u)
-        for j in range(n_tp):
-            tok_local(j).start()
         for u in FIRST + SHARED:
             local_w(u).start()
-        tok_local_wait()
+        tok_local_wait(1, n_tp - 1)
         squares(1)
 
         def scale_own(j, carry):
@@ -564,19 +569,18 @@
 
     @pl.when(is_end)
     def _():
+        tok_local_wait(0, 1)
         for h in range(2):
             to_stage(h).start()
         send_near(INNER)
         send_near(VALUE)
         end_tok().start()
         send_near(OUTER)
-        for j in range(n_tp):
-            tok_local(j).start()
         for u in SHARED:
             send_partner(u)
         for u in SHARED:
             local_w(u).start()
-        tok_local_wait()
+        tok_local_wait(1, n_tp - 1)
         squares(1)
         squares_copy().start()
         for u in SHARED:
@@ -698,6 +702,7 @@
     @pl.when(is_end)
     def _():
         relay_opp(last, (2, 3))
+        relay_far(last, (0, 1))
 
     @pl.when(is_mid)
     def _():
@@ -712,7 +717,7 @@
 
     @pl.when(is_end)
     def _():
-        relay_far(last)
+        relay_far(last, (2, 3))
     settle(GROUP + 4)
 
     def finish_last(cols):
@@ -804,7 +809,7 @@
             pltpu.VMEM((3, 16, chans), bf16),
             dma((2,)),
             dma,
-            dma,
+            dma((2,)),
             dma((2,)),
             dma((5,)),
             dma,

time: 98.8 us -> 98.4 us (level)
  no operation moved by 1% of the time
where the time goes in v8:
time: 98.4 us; the launch traced here: 98.2 us
  Pallas kernels  97.4 us (99%)
    pallas_call x1, Pallas kernels, fused(): pl.pallas_call(mixer_kernel, out_shape=jax.ShapeDtypeStruct((rows, feats)...  97.4 us

profile of v8, /device:TPU:1, one launch (start us, length us, event | category | flops | bytes accessed | tf_op | source)
XLA Modules:
  0.0 98.2 jit_solution(14605534087617199846)
XLA Ops:
  0.0 97.4 %mixer.1 = bf16[256,1024]{1,0:T(8,128)(2,1)S(1)} custom-call(bf16[256,4096]{1,0:T(8,128)(2,1)} %tok.1, f32[2,4096]{1,0:T(2,128)} %gain_hbm.1, bf16[2,512,256]{2,1,0:T(8,128)(2,1)} %w_outer.1, bf16[2,512,256]{2,1,0:T(8,128)(2,1)} %w_inner.1, bf16[2,512,256]{2,1,0:T(8,128)(2,1)} %w_value.1, bf16[2,128,1024]{2,1,0:T(8,128)(2,1)} %w_back.1, f32[3,2,256]{2,1,0:T(2,128)} %bitcast.1), custom_call_target="tpu_custom_call" | custom-call | tf_op jit(solution)/shard_map/mixer/pallas_call | solution.py:785
  97.4 0.8 copy.9

commit v9 on v8

--- a/solution.py
+++ b/solution.py
@@ -160,6 +160,9 @@
         )
 
     def piece(ref, u, k):
+        if u == 7:
+            size = ref.shape[1] // PIECES[u]
+            return ref.at[:, pl.ds(k * size, size)]
         size = ref.shape[0] // PIECES[u]
         return ref.at[pl.ds(k * size, size)]
 
@@ -174,7 +177,7 @@
     def to_partner(u, k, role):
         to = piece(held_w(u, source_of[role]), u, k)
         a = piece(own_w(u), u, k) if role == OWN else to
-        return remote(a, to, w_send.at[role // 2], p_recv.at[group_of(u, role)], partner, t)
+        return remote(a, to, w_send.at[role // 2], p_recv.at[group_of(u, role, k)], partner, t)
 
     def pieces_of(u):
         return range(PIECES[u])
@@ -220,19 +223,23 @@
     def relay_far(u, ks=None):
         relay_across(u, FAR, ks)
 
-    counts = {INNER: 2, VALUE: 2, OUTER: 2, BACK: 4, GROUP: 9, GROUP + 1: 1, GROUP + 2: 1, GROUP + 3: 1, 7: 3, GROUP + 4: 1}
-
-    def group_of(u, role):
+    counts = {INNER: 2, VALUE: 2, OUTER: 2, BACK: 4, GROUP: 9, GROUP + 1: 1, GROUP + 2: 1, GROUP + 3: 1, 7: 3}
+
+    def group_of(u, role, k):
         if u <= BACK:
             return u
         if u == 7:
-            return GROUP + 4 if role == FAR else 7
+            return GROUP + 4 + k if role == FAR else 7
         return GROUP + 1 + SECOND.index(u) if role == FAR else GROUP
 
     def settle(group):
         count = counts[group]
         ref = win.at[pl.ds(0, 3), pl.ds(0, 3)] if count == 9 else win.at[0, pl.ds(0, count)]
         remote(ref, ref, w_send.at[0], p_recv.at[group], partner, t).wait_recv()
+
+    def settle_last(k):
+        to = piece(held_w(7, far + flip), 7, k)
+        remote(to, to, w_send.at[0], p_recv.at[GROUP + 4 + k], partner, t).wait_recv()
 
     def sent(slot, planes_of, count):
         ref = win.at[pl.ds(0, planes_of), pl.ds(0, count)]
@@ -718,12 +725,14 @@
     @pl.when(is_end)
     def _():
         relay_far(last, (2, 3))
-    settle(GROUP + 4)
 
     def finish_last(cols):
         out[:, cols] = (bacc[:, cols] + back_dot(1, (FAR,), cols)).astype(bf16)
 
-    by_columns(finish_last)
+    size = feats // PIECES[last]
+    for k in pieces_of(last):
+        settle_last(k)
+        finish_last(pl.ds(k * size, size))
 
     some = units - 3
 
@@ -818,7 +827,7 @@
             dma,
             dma((2,)),
             dma((chunks,)),
-            dma((GROUP + 5,)),
+            dma((GROUP + 4 + PIECES[-1],)),
             dma((6,)),
             dma((6, 4)),
             dma((3,)),

time: 98.4 us -> 98.3 us (level)
  no operation moved by 1% of the time
where the time goes in v9:
time: 98.3 us; the launch traced here: 98 us
  Pallas kernels  97.2 us (99%)
    pallas_call x1, Pallas kernels, fused(): pl.pallas_call(mixer_kernel, out_shape=jax.ShapeDtypeStruct((rows, feats)...  97.2 us

profile of v9, /device:TPU:1, one launch (start us, length us, event | category | flops | bytes accessed | tf_op | source)
XLA Modules:
  0.0 98.0 jit_solution(14402956887680755489)
XLA Ops:
  0.0 97.2 %mixer.1 = bf16[256,1024]{1,0:T(8,128)(2,1)S(1)} custom-call(bf16[256,4096]{1,0:T(8,128)(2,1)} %tok.1, f32[2,4096]{1,0:T(2,128)} %gain_hbm.1, bf16[2,512,256]{2,1,0:T(8,128)(2,1)} %w_outer.1, bf16[2,512,256]{2,1,0:T(8,128)(2,1)} %w_inner.1, bf16[2,512,256]{2,1,0:T(8,128)(2,1)} %w_value.1, bf16[2,128,1024]{2,1,0:T(8,128)(2,1)} %w_back.1, f32[3,2,256]{2,1,0:T(2,128)} %bitcast.1), custom_call_target="tpu_custom_call" | custom-call | tf_op jit(solution)/shard_map/mixer/pallas_call | solution.py:794
  97.2 0.8 copy.9
